TPU v7x, 256 devices: a whole 4x4x8 slice. The times are simulated.
256 devices in a mesh: sp: 128 (over z, y, x), tp: 2 (over core).
Axes of the slice: x: 4, y: 4, z: 8, core: 2. Of those that a mesh axis runs over, the one named last changes fastest.
Arguments:
- conv_value: bfloat16 [65536, 1536], P('sp', 'tp'), may hold values from -6 to 6
- conv_gate: bfloat16 [65536, 1536], P('sp', 'tp'), may hold values from -8 to 8
- conv_out: bfloat16 [65536, 1536], P('sp', 'tp'), may hold values from -40 to 40
- conv_taps: bfloat16 [31, 1536], P(None, 'tp'), may hold values from -1 to 1
- norm_gain: float32 [1536], P('tp'), may hold values from 0.1 to 1.9
- norm_shift: float32 [1536], P('tp'), may hold values from -3 to 3
- proj_weight: bfloat16 [2048, 1536], P(None, 'tp'), may hold values from -0.15625 to 0.15625
- out_grad: bfloat16 [65536, 2048], P('sp'), may hold values from -24 to 24
Outputs:
- grad_value: bfloat16 [65536, 1536], P('sp', 'tp')
- grad_gate: bfloat16 [65536, 1536], P('sp', 'tp')
- grad_taps: float32 [31, 1536], P(None, 'tp')
- grad_gain: float32 [1536], P('tp')
- grad_shift: float32 [1536], P('tp')
- grad_proj: float32 [2048, 1536], P('sp', 'tp')
All inputs are finite; a program needn't handle non-finite values.
Results may differ from a plain program's by a relative error of at most 0.005.
Values may be sent and summed in bfloat16 or wider, within the bound.
A program may use at most 64 MiB of HBM per device.

v0:
```python
import functools

import jax
import jax.numpy as jnp
from jax import lax
from jax.sharding import Mesh
from jax.sharding import PartitionSpec as P

SP = ("sp_0", "sp_1", "sp_2")


norm_eps = 1e-05


def own_rows_2(running, axes):
    for axis in axes:
        running = lax.psum_scatter(running, axis, scatter_dimension=0, tiled=True)
    return running


def shifted_2(block, axis, distance):
    devices = range(lax.axis_size(axis))
    route = [(i - distance, i) for i in devices if i - distance in devices]
    return lax.ppermute(block, axis, route)


def one_axis_at_a_time(array, axes):
    return functools.reduce(lax.psum, axes, array)


def project_rows(out_grad, active):
    return own_rows_2(
        lax.dot_general(
            out_grad, active, (((0,), (0,)), ((), ())), preferred_element_type=jnp.float32
        ),
        SP,
    )


def local(conv_value, conv_gate, conv_out, conv_taps, norm_gain, norm_shift, proj_weight, out_grad):
    seq_rows, chan_local = conv_value.shape
    tap_reach = conv_taps.shape[0] - 1
    chan_total = chan_local * lax.axis_size("tp")
    height = conv_out.astype(jnp.float32)
    center = lax.psum(jnp.sum(height, axis=1), "tp") / chan_total
    centered = height - center[:, None]
    variance = lax.psum(jnp.sum(centered * centered, axis=1), "tp") / chan_total
    inv_std = lax.rsqrt(variance + norm_eps)[:, None]
    normed = centered * inv_std
    shifted = normed * norm_gain + norm_shift
    sig_norm = jax.nn.sigmoid(shifted)
    active = (shifted * sig_norm).astype(jnp.bfloat16)
    act_grad = jnp.dot(out_grad, proj_weight, preferred_element_type=jnp.float32)
    norm_grad = act_grad * (sig_norm * (1.0 + shifted * (1.0 - sig_norm)))
    scaled = norm_grad * norm_gain
    grad_sum, grad_dot = lax.psum((jnp.sum(scaled, axis=1), jnp.sum(scaled * normed, axis=1)), "tp")
    height_grad = inv_std * (
        scaled - grad_sum[:, None] / chan_total - normed * (grad_dot[:, None] / chan_total)
    )
    sig_gate = jax.nn.sigmoid(conv_gate.astype(jnp.float32))
    value_float = conv_value.astype(jnp.float32)
    gated_rows = (value_float * sig_gate).astype(jnp.bfloat16)
    tap_values = conv_taps.astype(jnp.float32)
    earlier = shifted_2(gated_rows[seq_rows - tap_reach :], SP, 1)
    extended = jnp.concatenate([earlier, gated_rows], axis=0).astype(jnp.float32)
    padded_grad = jnp.pad(height_grad, ((tap_reach, tap_reach), (0, 0)))
    spill_rows = jnp.zeros((seq_rows + tap_reach, chan_local), jnp.float32)
    for tap_index in range(tap_reach + 1):
        begin = tap_reach - tap_index
        spill_rows = (
            spill_rows + tap_values[tap_index] * padded_grad[begin : begin + seq_rows + tap_reach]
        )
    returned = shifted_2(spill_rows[:tap_reach], SP, -1)
    gated_grad = spill_rows[tap_reach:] + jnp.pad(returned, ((seq_rows - tap_reach, 0), (0, 0)))
    tap_rows = jnp.stack(
        [
            jnp.sum(height_grad * extended[tap_index : tap_index + seq_rows], axis=0)
            for tap_index in range(tap_reach + 1)
        ]
    )
    gain_row = jnp.sum(norm_grad * normed, axis=0)
    shift_row = jnp.sum(norm_grad, axis=0)
    grad_taps, grad_gain, grad_shift = (
        one_axis_at_a_time(tap_rows, SP),
        one_axis_at_a_time(gain_row, SP),
        one_axis_at_a_time(shift_row, SP),
    )
    grad_value = (gated_grad * sig_gate).astype(jnp.bfloat16)
    grad_gate = (gated_grad * value_float * sig_gate * (1.0 - sig_gate)).astype(jnp.bfloat16)
    grad_proj = project_rows(out_grad, active)
    return (grad_value, grad_gate, grad_taps, grad_gain, grad_shift, grad_proj)


def solution(mesh):
    split = Mesh(mesh.devices.reshape(8, 4, 4, mesh.shape["tp"]), ("sp_0", "sp_1", "sp_2", "tp"))
    placed = (
        P(SP, "tp"),
        P(SP, "tp"),
        P(SP, "tp"),
        P(None, "tp"),
        P("tp"),
        P("tp"),
        P(None, "tp"),
        P(SP, None),
    )
    return jax.shard_map(
        local,
        mesh=split,
        in_specs=placed,
        out_specs=(P(SP, "tp"), P(SP, "tp"), P(None, "tp"), P("tp"), P("tp"), P(SP, "tp")),
        check_vma=False,
    )
```

profile of v0, /device:TPU:2, one launch (start us, length us, event | category | flops | bytes accessed | tf_op | source)
XLA Modules:
  0.0 349.0 jit_solution(18354876950033820677)
XLA Ops:
  7.3 2.0 fusion.54
  9.2 0.9 copy-done.5
  10.1 3.4 collective-permute-start.1
  13.6 0.2 convert_reduce_fusion
  13.7 2.5 psum.91
  16.2 1.5 fusion.50
  17.7 2.5 psum.92
  20.2 5.4 %fusion.49 = (f32[768]{0:T(1024)S(1)}, f32[512]{0:T(512)S(1)}, f32[512]{0:T(512)S(1)}, f32[768]{0:T(1024)S(1)}, f32[512,768]{1,0:T(8,128)}) fusion(bf16[512,768]{1,0:T(8,128)(2,1)} %param.10, f32[512]{0:T(512)S(1)} %add_rsqrt_fusion, f32[512]{0:T(512)S(1)} %broadcast_multiply_fusion.2, f32[768]{0:T(1024)S(1)} %copy-done.8, f32[768]{0:T(1024)S(1)} %copy-done.9, ...), kind=kOutput, calls=%fused_computation.70 | convolution fusion | flops 1618474496 | bytes 7622656 | tf_op jit(solution)/shard_map/dot_general | solution.py:53
  25.6 2.4 all-reduce.5
  28.0 1.4 maximum_convert_fusion
  29.5 0.4 copy-done.6
  29.9 4.8 %fusion.55 = (f32[768]{0:T(1024)S(1)}, f32[768]{0:T(1024)S(1)}, f32[768]{0:T(1024)S(1)}, f32[768]{0:T(1024)S(1)}, f32[768]{0:T(1024)S(1)}, /*index=5*/f32[768]{0...) fusion(f32[542,768]{1,0:T(8,128)S(1)} %maximum_convert_fusion, ...), kind=kLoop, calls=%fused_computation.77 | loop fusion | flops 17287680 | bytes 32310272 | tf_op jit(solution)/shard_map/reduce_sum | solution.py:77
  34.7 2.5 fusion.73
  37.6 2.6 stack.127
  40.3 6.6 %convolution_bitcast_fusion = f32[2048,768]{0,1:T(8,128)} fusion(bf16[512,2048]{1,0:T(8,128)(2,1)} %param.15, bf16[512,768]{1,0:T(8,128)(2,1)} %param.10, f32[768]{0:T(1024)S(1)} %copy-done.9, f32[768]{0:T(1024)S(1)} %copy-done.8, f32[512]{0:T(512)S(1)} %add_rsqrt_fusion, f32[512]{0:T(512)S(1)} %broadcast_multiply_fusion.2), kind=kOutput, calls=%fused_computation | convolution fusion | flops 1614544896 | bytes 9185280 | tf_op jit(solution)/shard_map/dot_general | solution.py:33
  47.0 68.5 %all-reduce.10.cloned.1.call-done = f32[31,768]{1,0:T(8,128)} async-done(((f32[31,768]{1,0:T(8,128)}), f32[31,768]{1,0:T(8,128)}) %all-reduce.10.cloned.1.call-update) | async-done | bytes 95248 | tf_op jit(solution)/shard_map/psum | solution.py:28
  115.6 75.7 %reduce-scatter.8.cloned.1.call-done = f32[256,768]{0,1:T(8,128)} async-done(((f32[2048,768]{0,1:T(8,128)}), f32[256,768]{0,1:T(8,128)}) %reduce-scatter.8.cloned.1.call-update) | async-done | bytes 786448 | tf_op jit(solution)/shard_map/reduce_scatter | solution.py:17
  191.3 2.3 copy.16
  193.6 0.1 slice_reduce_fusion.29
  193.8 0.2 slice_reduce_fusion.30
  193.9 44.8 %all-reduce.12.cloned.1.call-done = f32[31,768]{1,0:T(8,128)} async-done(((f32[31,768]{1,0:T(8,128)}), f32[31,768]{1,0:T(8,128)}) %all-reduce.12.cloned.1.call-update) | async-done | bytes 95248 | tf_op jit(solution)/shard_map/psum | solution.py:28
  238.7 0.2 reduce-scatter.12.cloned.1.call-start
  238.9 25.3 %multiply_add_fusion = f32[542,768]{1,0:T(8,128)S(1)} fusion(f32[512,768]{1,0:T(8,128)} %copy-done.1, f32[768]{0:T(1024)S(1)} %get-tuple-element.54, f32[768]{0:T(1024)S(1)} %get-tuple-element.55, f32[768]{0:T(1024)S(1)} %get-tuple-element.56, f32[768]{0:T(1024)S(1)} %get-tuple-element.57, f32[768]{0:T(1024)S(1)} %get-tuple-element.58, ...), kind=kLoop, calls=%fused_computation.11 | loop fusion | flops 25391616 | bytes 3333120 | tf_op jit(solution)/shard_map/add | solution.py:71
  264.2 1.2 copy-done.4
  265.4 2.5 collective-permute-start
  267.9 17.7 %all-reduce.2 = (f32[768]{0:T(1024)S(1)}, f32[768]{0:T(1024)S(1)}) all-reduce(f32[768]{0:T(1024)S(1)} %get-tuple-element.49, f32[768]{0:T(1024)S(1)} %get-tuple-element.52), channel_id=1, replica_groups=mesh['sp_0'=8,'sp_1'=4,'sp_2'=4,'tp'=2] {'sp_0'}, use_global_device_ids=true, to_apply=%region_43.44 | all-reduce | flops 1536 | bytes 12288 | tf_op jit(solution)/shard_map/psum | solution.py:28
  285.6 9.4 %all-reduce.4 = (f32[768]{0:T(1024)S(1)}, f32[768]{0:T(1024)S(1)}) all-reduce(f32[768]{0:T(1024)S(1)} %get-tuple-element.84, f32[768]{0:T(1024)S(1)} %get-tuple-element.85), channel_id=1, replica_groups=mesh['sp_0'=8,'sp_1'=4,'sp_2'=4,'tp'=2] {'sp_1'}, use_global_device_ids=true, to_apply=%region_44.45 | all-reduce | flops 1536 | bytes 12288 | tf_op jit(solution)/shard_map/psum | solution.py:28
  295.0 11.7 %all-reduce.3 = (f32[768]{0:T(1024)}, f32[768]{0:T(1024)}) all-reduce(f32[768]{0:T(1024)S(1)} %get-tuple-element.88, f32[768]{0:T(1024)S(1)} %get-tuple-element.89), channel_id=1, replica_groups=mesh['sp_0'=8,'sp_1'=4,'sp_2'=4,'tp'=2] {'sp_2'}, use_global_device_ids=true, to_apply=%region_45.46 | all-reduce | flops 1536 | bytes 12288 | tf_op jit(solution)/shard_map/psum | solution.py:28
  306.7 3.7 %fusion.53 = (bf16[512,768]{1,0:T(8,128)(2,1)}, bf16[512,768]{1,0:T(8,128)(2,1)}) fusion(bf16[512,768]{1,0:T(8,128)(2,1)} %param.8, f32[30,768]{1,0:T(8,128)S(1)} %collective-permute-done, f32[542,768]{1,0:T(8,128)} %copy-done.4, bf16[512,768]{1,0:T(8,128)(2,1)} %param.9), kind=kLoop, calls=%fused_computation.74 | loop fusion | flops 5111808 | bytes 4810752 | tf_op jit(solution)/shard_map/convert_element_type | solution.py:89
  310.5 4.1 %all-reduce.14.cloned.1.call-done = f32[31,768]{1,0:T(8,128)} async-done(((f32[31,768]{1,0:T(8,128)}), f32[31,768]{1,0:T(8,128)}) %all-reduce.14.cloned.1.call-update) | async-done | bytes 95248 | tf_op jit(solution)/shard_map/psum | solution.py:28
  314.6 26.0 %reduce-scatter.12.cloned.1.call-done = f32[16,768]{1,0:T(8,128)} async-done(((f32[64,768]{1,0:T(8,128)}), f32[16,768]{1,0:T(8,128)}) %reduce-scatter.12.cloned.1.call-update) | async-done | bytes 49168
  340.6 1.5 copy.23
  (68 shorter events, 0.5 us)
Async XLA Ops:
  7.2 13.0 %copy-start = (bf16[2048,768]{1,0:T(8,128)(2,1)S(1)}, bf16[2048,768]{1,0:T(8,128)(2,1)}, u32[]{:S(2)}) copy-start(bf16[2048,768]{1,0:T(8,128)(2,1)} %param.14) | copy-start | bytes 9437188
  7.2 13.0 %copy-start.8 = (f32[768]{0:T(1024)S(1)}, f32[768]{0:T(1024)}, u32[]{:S(2)}) copy-start(f32[768]{0:T(1024)} %param.12) | copy-start | bytes 9220
  7.2 13.0 %copy-start.9 = (f32[768]{0:T(1024)S(1)}, f32[768]{0:T(1024)}, u32[]{:S(2)}) copy-start(f32[768]{0:T(1024)} %param.13) | copy-start | bytes 9220
  7.2 108.3 %all-reduce.10.cloned.1.call-start = ((), (), s32[]{:S(2)}) async-start(), calls=%async_computation.3 | async-start | bytes 196608 | tf_op jit(solution)/shard_map/psum | solution.py:28
  7.2 6.3 %copy-start.2 = (bf16[512,768]{1,0:T(8,128)(2,1)S(1)}, bf16[512,768]{1,0:T(8,128)(2,1)}, u32[]{:S(2)}) copy-start(bf16[512,768]{1,0:T(8,128)(2,1)} %param.10) | copy-start | bytes 2359300
  9.2 0.9 copy-start.5
  10.1 17.9 %collective-permute-start.1 = (bf16[30,768]{1,0:T(8,128)(2,1)S(1)}, bf16[30,768]{1,0:T(8,128)(2,1)S(1)}, u32[]{:S(2)}, u32[]{:S(2)}) collective-permute-start(bf16[30,768]{1,0:T(8,128)(2,1)S(1)} %slice.417), channel_id=1, source_target_pairs={{0,2},{2,4},{4,6},{6,8},{8,10},{10,12},{12,14},{14,16},{16,18},{18... | collective-permute-start | bytes 138248 | tf_op jit(solution)/shard_map/ppermute | solution.py:24
  28.0 1.5 copy-start.3
  28.0 1.9 copy-start.6
  34.7 2.6 copy-start.1
  40.3 151.0 %reduce-scatter.8.cloned.1.call-start = ((), (), s32[]{:S(2)}) async-start(), calls=%async_computation.6 | async-start | bytes 7077888 | tf_op jit(solution)/shard_map/reduce_scatter | solution.py:17
  46.9 146.7 %copy-start.7 = (bf16[31,768]{1,0:T(8,128)(2,1)S(1)}, bf16[31,768]{1,0:T(8,128)(2,1)}, u32[]{:S(2)}) copy-start(bf16[31,768]{1,0:T(8,128)(2,1)} %param.11) | copy-start | bytes 142852
  46.9 191.8 %all-reduce.12.cloned.1.call-start = ((), (), s32[]{:S(2)}) async-start(), calls=%async_computation.4 | async-start | bytes 196608 | tf_op jit(solution)/shard_map/psum | solution.py:28
  115.5 191.2 %reduce-scatter.10.cloned.1.call-start = ((), (), s32[]{:S(2)}) async-start(), calls=%async_computation.7 | async-start | bytes 983040
  193.6 121.0 %all-reduce.14.cloned.1.call-start = ((), (), s32[]{:S(2)}) async-start(), calls=%async_computation.5 | async-start | bytes 196608 | tf_op jit(solution)/shard_map/psum | solution.py:28
  238.7 101.9 %reduce-scatter.12.cloned.1.call-start = ((), (), s32[]{:S(2)}) async-start(), calls=%async_computation.8 | async-start | bytes 245760
  264.2 1.2 copy-start.4
  265.4 41.3 %collective-permute-start = (f32[30,768]{1,0:T(8,128)S(1)}, f32[30,768]{1,0:T(8,128)S(1)}, u32[]{:S(2)}, u32[]{:S(2)}) collective-permute-start(f32[30,768]{1,0:T(8,128)S(1)} %slice.416), channel_id=1, source_target_pairs={{2,0},{4,2},{6,4},{8,6},{10,8},{12,10},{14,12},{16,14},{18,16},{20... | collective-permute-start | bytes 276488 | tf_op jit(solution)/shard_map/ppermute | solution.py:24
Sparse Core Ops, SparseCore 0:
  40.4 75.0 all-reduce.9
  118.1 73.1 reduce-scatter.7
  193.6 45.0 all-reduce.11
  241.7 25.6 reduce-scatter.9
  269.5 44.9 all-reduce.13
  317.5 23.0 reduce-scatter.11
where the time goes:
time: 351 us; the launch traced here: 349 us
  waiting for transfers between devices  219 us (62%)
  blocking collectives  46.2 us (13%)
  other arithmetic  41.4 us (12%)
  between operations  14.6 us (4%)
  matrix products  11.9 us (3%)
  local copies, waits for them, and re-layouts  9.34 us (3%)
  starting transfers between devices  6.28 us (2%)
    psum x3, waiting for transfers between devices, one_axis_at_a_time(): return functools.reduce(lax.psum, axes, array)  117 us
    reduce_scatter x1, waiting for transfers between devices, own_rows_2(): running = lax.psum_scatter(running, axis, scatter_dimension=0, tiled=True)  75.7 us
    psum x3, blocking collectives, one_axis_at_a_time(): return functools.reduce(lax.psum, axes, array)  38.8 us
    unnamed x8, waiting for transfers between devices  26.1 us
    add x1, other arithmetic, local(): spill_rows + tap_values[tap_index] * padded_grad[begin:begin + seq_rows +...  25.3 us
    reduce_sum x2, other arithmetic, local(): jnp.sum(height_grad * extended[tap_index:tap_index + seq_rows], axis=0)  7.32 us
  transfers between devices with their start and end apart: 8, of which 5 were waited for; matrix products, arithmetic and copies ran while one was open for 13% of the time, Pallas kernels for 0%

commit v1 on v0

v1 whole, which is shorter than its diff:
```python
import jax
import jax.numpy as jnp
from jax import lax
from jax.experimental import pallas as pl
from jax.experimental.pallas import tpu as pltpu
from jax.sharding import Mesh
from jax.sharding import PartitionSpec as P

SP = ("sp_0", "sp_1", "sp_2")
MESH = pl.DeviceIdType.MESH
F32, BF16 = jnp.float32, jnp.bfloat16

norm_eps = 1e-05
LANES = 128
HALO = 32
AUX = 40
NX = NY = 4
NZ = 8
PLANE = NX * NY


def sigmoid(v):
    return 0.5 + 0.5 * jnp.tanh(0.5 * v)


def kernel(
    value_h, gate_h, out_h, taps_h, gain_h, shift_h, weight_h, og_h,
    gv_h, gg_h, gtaps_o, ggain_o, gshift_o, gproj_o,
    value_v, gate_v, out_v, taps_v, gain_v, shift_v, weight_v, og_v, in_sem,
    st_a, st_b, cen_b, inv_b, act_v, fac_v, sc_v, hg, gt, tapsf,
    gx, r1x, r2x, r3x, mx, hx, s1x, s2x, s3x, mx2, ex, zx,
    gy, r1y, r2y, r3y, my, hy, s1y, s2y, s3y, my2, ey, zy,
    red, red_r, zred, ag,
    st_sem, halo_sem, rs_send, rs_recv, z_send, z_recv, ar_send, ar_recv, gv_v, gg_v, out_sem,
):
    rows, chans = value_v.shape
    groups = chans // LANES
    taps_n = taps_v.shape[0]
    reach = taps_n - 1
    chan_total = 2.0 * chans
    z, y, x = (lax.axis_index(a) for a in SP)
    core = lax.axis_index("tp")
    place = (z * NY + y) * NX + x
    last = NZ * PLANE

    def at_place(s):
        return {"sp_0": s // PLANE, "sp_1": lax.rem(s // NX, NY), "sp_2": lax.rem(s, NX)}

    nxt = at_place(lax.rem(place + 1, last))
    prv = at_place(lax.rem(place + last - 1, last))

    def load(i, src, dst):
        c = pltpu.make_async_copy(src, dst, in_sem.at[i])
        c.start()
        return c

    def send(src, dst, ss, rs, dev):
        c = pltpu.make_async_remote_copy(
            src_ref=src, dst_ref=dst, send_sem=ss, recv_sem=rs, device_id=dev, device_id_type=MESH
        )
        c.start()
        return c

    c_out = load(0, out_h, out_v)
    c_gain = load(1, gain_h, gain_v)
    c_shift = load(2, shift_h, shift_v)
    c_taps = load(3, taps_h, taps_v)

    barrier = pltpu.get_barrier_semaphore()
    partners = [{"tp": 1 - core}, nxt, prv]
    p_me = y * NX + x
    plane_dev = []
    plane_pos = []
    for k in range(1, PLANE):
        p = lax.rem(p_me + k, PLANE)
        plane_pos.append(p)
        plane_dev.append({"sp_1": p // NX, "sp_2": lax.rem(p, NX)})
    z_pos = [lax.rem(z + k, NZ) for k in range(1, NZ)]
    z_dev = [{"sp_0": p} for p in z_pos]
    partners += plane_dev + z_dev
    for dev in partners:
        pl.semaphore_signal(barrier, inc=1, device_id=dev, device_id_type=MESH)

    c_out.wait()
    c_gate = load(4, gate_h, gate_v)
    c_value = load(5, value_h, value_v)
    c_og = load(6, og_h, og_v)
    c_weight = load(7, weight_h, weight_v)

    def cols(g):
        return slice(g * LANES, (g + 1) * LANES)

    SB = 64

    @pl.loop(0, rows // SB)
    def _(i):
        rs = pl.ds(i * SB, SB)
        v = out_v[rs, :].astype(F32)
        s = jnp.sum(v, axis=1, keepdims=True)
        d = v - s * (1.0 / chans)
        m2 = jnp.sum(d * d, axis=1, keepdims=True)
        lane = lax.broadcasted_iota(jnp.int32, (SB, LANES), 1)
        st_a[0, rs, :] = jnp.where(lane < LANES // 2, s, m2)

    pl.semaphore_wait(barrier, len(partners))
    c_st1 = send(st_a.at[0], st_b.at[0], st_sem.at[0], st_sem.at[1], {"tp": 1 - core})

    c_gate.wait()
    c_value.wait()

    @pl.loop(0, rows // SB)
    def _(i):
        rs = pl.ds(i * SB, SB)
        for g in range(groups):
            gated = value_v[rs, cols(g)].astype(F32) * sigmoid(gate_v[rs, cols(g)].astype(F32))
            gt[g, pl.ds(HALO + i * SB, SB), :] = gated.astype(BF16).astype(F32)

    c_gain.wait()
    c_shift.wait()
    c_taps.wait()
    for g in range(groups):
        tapsf[g, 0:taps_n, :] = taps_v[:, cols(g)].astype(F32)
    c_halo = send(
        gt.at[:, pl.ds(rows, HALO), :], gt.at[:, pl.ds(0, HALO), :],
        halo_sem.at[0], halo_sem.at[1], nxt,
    )
    c_st1.wait()

    @pl.loop(0, rows // SB)
    def _(i):
        rs = pl.ds(i * SB, SB)
        own, peer = st_a[0, rs, :], st_b[0, rs, :]
        s0, m0 = own[:, 0:1], own[:, LANES // 2 : LANES // 2 + 1]
        s1, m1 = peer[:, 0:1], peer[:, LANES // 2 : LANES // 2 + 1]
        ds = s0 - s1
        var = (m0 + m1 + ds * ds * (1.0 / chan_total)) * (1.0 / chan_total)
        inv = lax.rsqrt(var + norm_eps)
        cen = (s0 + s1) * (1.0 / chan_total)
        cen_b[rs, :] = jnp.broadcast_to(cen, (SB, LANES))
        inv_b[rs, :] = jnp.broadcast_to(inv, (SB, LANES))
        for g in range(groups):
            gain = gain_v[:, cols(g)]
            shift = shift_v[:, cols(g)]
            sh = (out_v[rs, cols(g)].astype(F32) - cen) * inv * gain + shift
            sg = sigmoid(sh)
            act_v[rs, cols(g)] = (sh * sg).astype(BF16)
            fac_v[rs, cols(g)] = sg * (1.0 + sh * (1.0 - sg))

    c_og.wait()
    zb = PLANE * 16
    half_c = chans // 2

    @pl.loop(0, NZ)
    def _(zz):
        lhs = og_v[:, pl.ds(pl.multiple_of(zz * zb, zb), zb)]
        part = lax.dot_general(
            lhs, act_v[...], (((0,), (0,)), ((), ())), preferred_element_type=F32
        ).astype(BF16)
        hf, zq = zz // (NZ // 2), lax.rem(zz, NZ // 2)
        for yy in range(NY):
            for xx in range(NX):
                r0 = (yy * NX + xx) * 16
                gx[xx, hf, yy * 4 + zq] = part[r0 : r0 + 16, 0:half_c]
                gy[yy, hf, xx * 4 + zq] = part[r0 : r0 + 16, half_c:]

    DIRS = (1, -1)

    def ring_start(g, r1, r3, axis, pos, base):
        out = []
        for h, d in enumerate(DIRS):
            out.append(send(
                g.at[lax.rem(pos + 2, 4), h], r1.at[h],
                rs_send.at[base + h], rs_recv.at[base + h], {axis: lax.rem(pos + 4 + d, 4)},
            ))
        for h, d in enumerate(DIRS):
            out.append(send(
                g.at[lax.rem(pos + 4 - d, 4), h], r3.at[h],
                rs_send.at[base + 2 + h], rs_recv.at[base + 2 + h], {axis: lax.rem(pos + 4 - d, 4)},
            ))
        return out

    def ring_mid(g, r1, m, r2, first, axis, pos, base):
        out = []
        for h, d in enumerate(DIRS):
            first[h].wait_recv()
            idx = lax.rem(pos + 4 + d, 4)

            @pl.loop(0, r1.shape[1])
            def _(j, h=h, idx=idx):
                m[h, j] = (r1[h, j].astype(F32) + g[idx, h, j].astype(F32)).astype(BF16)

            out.append(send(
                m.at[h], r2.at[h],
                rs_send.at[base + 4 + h], rs_recv.at[base + 4 + h], {axis: idx},
            ))
        return out

    def ring_end(g, r2, r3, first, second, pos, write):
        for h in range(2):
            second[h].wait_recv()
            first[2 + h].wait_recv()

            @pl.loop(0, r2.shape[1])
            def _(j, h=h):
                t = r2[h, j].astype(F32) + r3[h, j].astype(F32) + g[pos, h, j].astype(F32)
                write(h, j, t.astype(BF16))

    fx = ring_start(gx, r1x, r3x, "sp_2", x, 0)
    fy = ring_start(gy, r1y, r3y, "sp_1", y, 6)

    c_weight.wait()
    NB = 256

    @pl.loop(0, chans // NB)
    def _(n):
        cs = pl.ds(pl.multiple_of(n * NB, NB), NB)
        sc_v[:, cs] = jnp.dot(og_v[...], weight_v[:, cs], preferred_element_type=F32)

    zero = jnp.zeros((8, LANES), F32)

    def norm_pass(i, carry):
        rs = pl.ds(i * SB, SB)
        cen, inv = cen_b[rs, :], inv_b[rs, :]
        r_sum = jnp.zeros((SB, LANES), F32)
        r_dot = jnp.zeros((SB, LANES), F32)
        new = []
        for g in range(groups):
            n = sc_v[rs, cols(g)] * fac_v[rs, cols(g)]
            xc = (out_v[rs, cols(g)].astype(F32) - cen) * inv
            nx = n * xc
            new.append(carry[2 * g] + jnp.sum(nx.reshape(SB // 8, 8, LANES), axis=0))
            new.append(carry[2 * g + 1] + jnp.sum(n.reshape(SB // 8, 8, LANES), axis=0))
            sc = n * gain_v[:, cols(g)]
            r_sum = r_sum + sc
            r_dot = r_dot + sc * xc
            sc_v[rs, cols(g)] = sc
        lane = lax.broadcasted_iota(jnp.int32, (SB, LANES), 1)
        st_a[1, rs, :] = jnp.where(
            lane < LANES // 2,
            jnp.sum(r_sum, axis=1, keepdims=True),
            jnp.sum(r_dot, axis=1, keepdims=True),
        )
        return tuple(new)

    sums = lax.fori_loop(0, rows // SB, norm_pass, (zero,) * (2 * groups))
    c_st2 = send(st_a.at[1], st_b.at[1], st_sem.at[2], st_sem.at[3], {"tp": 1 - core})

    def put_row(g, j, row):
        red[(g * AUX + j) // 8, j % 8 : j % 8 + 1, :] = row

    for g in range(groups):
        put_row(g, taps_n, jnp.sum(sums[2 * g], axis=0, keepdims=True))
        put_row(g, taps_n + 1, jnp.sum(sums[2 * g + 1], axis=0, keepdims=True))
        for j in range(taps_n + 2, AUX):
            put_row(g, j, jnp.zeros((1, LANES), F32))
    for t in range(groups * AUX // 8, red.shape[0]):
        red[t] = zero
    c_st2.wait()

    @pl.loop(0, rows // SB)
    def _(i):
        rs = pl.ds(i * SB, SB)
        both = st_a[1, rs, :] + st_b[1, rs, :]
        gs = both[:, 0:1] * (1.0 / chan_total)
        gd = both[:, LANES // 2 : LANES // 2 + 1] * (1.0 / chan_total)
        cen, inv = cen_b[rs, :], inv_b[rs, :]
        for g in range(groups):
            xc = (out_v[rs, cols(g)].astype(F32) - cen) * inv
            hg[g, rs, :] = inv * (sc_v[rs, cols(g)] - gs - xc * gd)

    c_back = send(
        hg.at[:, pl.ds(0, HALO), :], hg.at[:, pl.ds(rows, HALO), :],
        halo_sem.at[2], halo_sem.at[3], prv,
    )

    mid_x = ring_mid(gx, r1x, mx, r2x, fx, "sp_2", x, 0)
    mid_y = ring_mid(gy, r1y, my, r2y, fy, "sp_1", y, 6)

    c_halo.wait_recv()

    @pl.when(place == 0)
    def _():
        gt[:, 0:HALO, :] = jnp.zeros((groups, HALO, LANES), F32)

    @pl.loop(0, groups)
    def _(g):
        def step(t, acc):
            h = hg[g, pl.ds(pl.multiple_of(t * 8, 8), 8), :]
            return tuple(
                acc[j] + h * gt[g, pl.ds(t * 8 + (HALO - reach + j), 8), :] for j in range(taps_n)
            )

        acc = lax.fori_loop(0, rows // 8, step, (zero,) * taps_n)
        for j in range(taps_n):
            red[g * (AUX // 8) + j // 8, j % 8 : j % 8 + 1, :] = jnp.sum(
                acc[j], axis=0, keepdims=True
            )

    ar_a = []
    for k in range(1, PLANE):
        ar_a.append(send(
            red.at[pl.ds(2 * plane_pos[k - 1], 2)], red_r.at[k - 1],
            ar_send.at[k - 1], ar_recv.at[k - 1], plane_dev[k - 1],
        ))

    c_back.wait_recv()

    @pl.when(place == last - 1)
    def _():
        hg[:, rows : rows + HALO, :] = jnp.zeros((groups, HALO, LANES), F32)

    TB = 16

    def gated_part(g):
        weights = [jnp.broadcast_to(tapsf[g, j : j + 1, :], (8, LANES)) for j in range(taps_n)]

        @pl.loop(0, rows // TB)
        def _(t):
            parts = []
            for b in range(TB // 8):
                acc = [None, None]
                for j in range(taps_n):
                    term = weights[j] * hg[g, pl.ds(t * TB + (b * 8 + reach - j), 8), :]
                    acc[j % 2] = term if acc[j % 2] is None else acc[j % 2] + term
                parts.append(acc[0] + acc[1])
            gg = jnp.concatenate(parts, axis=0)
            rs = pl.ds(pl.multiple_of(t * TB, TB), TB)
            sg = sigmoid(gate_v[rs, cols(g)].astype(F32))
            val = value_v[rs, cols(g)].astype(F32)
            gs = gg * sg
            gv_v[rs, cols(g)] = gs.astype(BF16)
            gg_v[rs, cols(g)] = (gs * val * (1.0 - sg)).astype(BF16)

        a = pltpu.make_async_copy(gv_v.at[:, cols(g)], gv_h.at[:, cols(g)], out_sem.at[2 * g])
        b = pltpu.make_async_copy(gg_v.at[:, cols(g)], gg_h.at[:, cols(g)], out_sem.at[2 * g + 1])
        a.start()
        b.start()
        return [a, b]

    outs = []
    for g in range(groups // 2):
        outs += gated_part(g)

    def to_x(h, j, v):
        hx[j // (NZ // 2), h, lax.rem(j, NZ // 2)] = v

    def to_y(h, j, v):
        hy[j // (NZ // 2), h, lax.rem(j, NZ // 2)] = v

    ring_end(gx, r2x, r3x, fx, mid_x, x, to_x)
    f2x = ring_start(hx, s1x, s3x, "sp_1", y, 12)
    ring_end(gy, r2y, r3y, fy, mid_y, y, to_y)
    f2y = ring_start(hy, s1y, s3y, "sp_2", x, 18)

    for g in range(groups // 2, groups):
        outs += gated_part(g)

    for c in ar_a:
        c.wait_recv()

    mine = red[pl.ds(2 * p_me, 2)]
    for k in range(PLANE - 1):
        mine = mine + red_r[k]
    zred[z] = mine
    ar_b = []
    for k in range(1, NZ):
        ar_b.append(send(
            zred.at[z], zred.at[z], ar_send.at[PLANE + k], ar_recv.at[PLANE + k], z_dev[k - 1],
        ))

    m2x = ring_mid(hx, s1x, mx2, s2x, f2x, "sp_1", y, 12)
    m2y = ring_mid(hy, s1y, my2, s2y, f2y, "sp_2", x, 18)

    for c in ar_b:
        c.wait_recv()
    total = zred[0]
    for k in range(1, NZ):
        total = total + zred[k]
    ag[pl.ds(2 * p_me, 2)] = total
    ar_c = []
    for k in range(1, PLANE):
        ar_c.append(send(
            ag.at[pl.ds(2 * p_me, 2)], ag.at[pl.ds(2 * p_me, 2)],
            ar_send.at[PLANE + NZ + k], ar_recv.at[PLANE + NZ + k], plane_dev[k - 1],
        ))

    def e_x(h, j, v):
        ex[h * (NZ // 2) + j] = v

    def e_y(h, j, v):
        ey[h * (NZ // 2) + j] = v

    ring_end(hx, s2x, s3x, f2x, m2x, y, e_x)
    ring_end(hy, s2y, s3y, f2y, m2y, x, e_y)
    zs = []
    for c, (e, zr) in enumerate(((ex, zx), (ey, zy))):
        for k in range(1, NZ):
            zs.append(send(
                e.at[z_pos[k - 1]], zr.at[k - 1],
                z_send.at[c * NZ + k], z_recv.at[c * NZ + k], z_dev[k - 1],
            ))

    for c in ar_c:
        c.wait_recv()
    for g in range(groups):
        for u in range(AUX // 8):
            tile = ag[g * (AUX // 8) + u]
            if u < taps_n // 8:
                gtaps_o[u * 8 : u * 8 + 8, cols(g)] = tile
            elif u == taps_n // 8:
                gtaps_o[u * 8 : taps_n, cols(g)] = tile[0 : taps_n - u * 8]
        for j, o in ((taps_n, ggain_o), (taps_n + 1, gshift_o)):
            o[:, cols(g)] = ag[(g * AUX + j) // 8, j % 8 : j % 8 + 1, :]

    for c in zs:
        c.wait_recv()
    for c, (e, zr) in enumerate(((ex, zx), (ey, zy))):
        t = e[z].astype(F32)
        for k in range(NZ - 1):
            t = t + zr[k].astype(F32)
        gproj_o[:, c * half_c : (c + 1) * half_c] = t

    for c in [c_halo, c_back, *fx, *fy, *mid_x, *mid_y, *f2x, *f2y, *m2x, *m2y, *ar_a, *ar_b, *ar_c, *zs]:
        c.wait_send()
    for c in outs:
        c.wait()


def local(conv_value, conv_gate, conv_out, conv_taps, norm_gain, norm_shift, proj_weight, out_grad):
    rows, chans = conv_value.shape
    taps_n = conv_taps.shape[0]
    d_model = proj_weight.shape[0]
    groups = chans // LANES
    half = chans // 2
    any_s = pl.BlockSpec(memory_space=pl.ANY)
    vm_s = pl.BlockSpec(memory_space=pltpu.VMEM)
    V = pltpu.VMEM
    DMA = pltpu.SemaphoreType.DMA

    def color():
        unit, small = (2, 16, 16, half), (2, 4, 16, half)
        return [
            V((4, 2, 16, 16, half), BF16),
            V(unit, BF16), V(unit, BF16), V(unit, BF16), V(unit, BF16),
            V((4, 2, 4, 16, half), BF16),
            V(small, BF16), V(small, BF16), V(small, BF16), V(small, BF16),
            V((8, 16, half), BF16),
            V((7, 16, half), BF16),
        ]

    scratch = [
        V((rows, chans), BF16), V((rows, chans), BF16), V((rows, chans), BF16),
        V((taps_n, chans), BF16), V((1, chans), F32), V((1, chans), F32),
        V((d_model, chans), BF16), V((rows, d_model), BF16), DMA((8,)),
        V((2, rows, LANES), F32), V((2, rows, LANES), F32), V((rows, LANES), F32), V((rows, LANES), F32),
        V((rows, chans), BF16), V((rows, chans), F32), V((rows, chans), F32),
        V((groups, rows + HALO, LANES), F32), V((groups, rows + HALO, LANES), F32),
        V((groups, 32, LANES), F32),
        *color(), *color(),
        V((32, 8, LANES), F32), V((PLANE - 1, 2, 8, LANES), F32), V((NZ, 2, 8, LANES), F32),
        V((32, 8, LANES), F32),
        DMA((4,)), DMA((4,)), DMA((24,)), DMA((24,)), DMA((2 * NZ,)), DMA((2 * NZ,)),
        DMA((2 * PLANE + NZ,)), DMA((2 * PLANE + NZ,)),
        V((rows, chans), BF16), V((rows, chans), BF16), DMA((2 * groups,)),
    ]
    S = jax.ShapeDtypeStruct
    gv, gg, gtaps, ggain, gshift, gproj = pl.pallas_call(
        kernel,
        name="conv_backward",
        out_shape=(
            S((rows, chans), BF16), S((rows, chans), BF16), S((taps_n, chans), F32),
            S((1, chans), F32), S((1, chans), F32), S((16, chans), F32),
        ),
        in_specs=[any_s] * 8,
        out_specs=(any_s, any_s, vm_s, vm_s, vm_s, vm_s),
        scratch_shapes=scratch,
        compiler_params=pltpu.CompilerParams(
            collective_id=0, has_side_effects=True, vmem_limit_bytes=56 * 1024 * 1024
        ),
    )(
        conv_value, conv_gate, conv_out, conv_taps,
        norm_gain.reshape(1, chans), norm_shift.reshape(1, chans), proj_weight, out_grad,
    )
    return gv, gg, gtaps, ggain.reshape(chans), gshift.reshape(chans), gproj


def solution(mesh):
    split = Mesh(mesh.devices.reshape(8, 4, 4, mesh.shape["tp"]), (*SP, "tp"))
    placed = (
        P(SP, "tp"), P(SP, "tp"), P(SP, "tp"), P(None, "tp"),
        P("tp"), P("tp"), P(None, "tp"), P(SP, None),
    )
    return jax.shard_map(
        local,
        mesh=split,
        in_specs=placed,
        out_specs=(P(SP, "tp"), P(SP, "tp"), P(None, "tp"), P("tp"), P("tp"), P(SP, "tp")),
        check_vma=False,
    )
```

time: 351 us -> 66.9 us (0.19)
  the two profiles are of different devices: /device:TPU:2 before, /device:TPU:6 now
where the time goes in v1:
time: 66.9 us; the launch traced here: 66.6 us
  Pallas kernels  55.4 us (83%)
  local copies, waits for them, and re-layouts  7.93 us (12%)
  other arithmetic  2.6 us (4%)
    pallas_call x1, Pallas kernels, local(): pl.pallas_call(kernel, name='conv_backward', out_shape=(S((rows, chans),...  55.4 us
    unnamed x8, local copies, waits for them, and re-layouts  5.39 us
    pallas_call x2, other arithmetic, local(): pl.pallas_call(kernel, name='conv_backward', out_shape=(S((rows, chans),...  2.6 us

profile of v1, /device:TPU:6, one launch (start us, length us, event | category | flops | bytes accessed | tf_op | source)
XLA Modules:
  0.0 66.6 jit_solution(13102918554003754170)
XLA Ops:
  0.6 1.3 %reshape.24.gain_h = f32[1,768]{1,0:T(1,128)} reshape(f32[768]{0:T(1024)} %param.12) | data formatting | bytes 6144 | tf_op jit(solution)/shard_map/reshape | solution.py:482
  1.9 1.3 %reshape.25.shift_h = f32[1,768]{1,0:T(1,128)} reshape(f32[768]{0:T(1024)} %param.13) | data formatting | bytes 6144 | tf_op jit(solution)/shard_map/reshape | solution.py:482
  3.2 55.4 %conv_backward.1 = (bf16[512,768]{1,0:T(8,128)(2,1)}, bf16[512,768]{1,0:T(8,128)(2,1)}, f32[31,768]{1,0:T(8,128)}, f32[1,768]{1,0:T(1,128)}, f32[1,768]{1,0:T(1,128)}, /*index=5*/f32[16,768]{1,0:T(8,128)}) custom-call(bf16[512,768]{1,0:T(8,128)(2,1)} %value_h.1, bf16[512,768]{1,0:T(8,128)(2,1)} %gate_h.1, bf16[512,768]{1,0:T(8,128)(2,1)} %out_h.1, ...), custom_call_target="tpu_custom_call" | custom-call | tf_op jit(solution)/shard_map/conv_backward/pallas_call | solution.py:467
  58.6 0.0 copy-start
  58.6 0.0 copy-start.1
  58.6 1.3 %reduce = f32[768]{0:T(1024)} reduce(f32[1,768]{1,0:T(1,128)} %get-tuple-element.15, f32[]{:T(128)} %constant), dimensions={0}, to_apply=%get-tuple-element.15.reduce_sub_computation | reduce | bytes 6148 | tf_op jit(solution)/shard_map/conv_backward/pallas_call | solution.py:467
  59.9 1.3 %reduce.1 = f32[768]{0:T(1024)} reduce(f32[1,768]{1,0:T(1,128)} %get-tuple-element.16, f32[]{:T(128)} %constant), dimensions={0}, to_apply=%get-tuple-element.16.reduce_sub_computation | reduce | bytes 6148 | tf_op jit(solution)/shard_map/conv_backward/pallas_call | solution.py:467
  61.2 2.1 %copy.18 = bf16[512,768]{1,0:T(8,128)(2,1)} copy(bf16[512,768]{1,0:T(8,128)(2,1)} %get-tuple-element.24) | data formatting | bytes 1572864
  63.3 2.1 %copy.19 = bf16[512,768]{1,0:T(8,128)(2,1)} copy(bf16[512,768]{1,0:T(8,128)(2,1)} %get-tuple-element.25) | data formatting | bytes 1572864
  65.3 0.0 copy-done
  65.3 0.6 copy.20
  66.0 0.0 copy-done.1
  66.0 0.6 copy.21
Async XLA Ops:
  58.6 6.7 %copy-start = (f32[31,768]{1,0:T(8,128)S(1)}, f32[31,768]{1,0:T(8,128)}, u32[]{:S(2)}) copy-start(f32[31,768]{1,0:T(8,128)} %get-tuple-element.26) | copy-start | bytes 285700
  58.6 7.4 %copy-start.1 = (f32[16,768]{1,0:T(8,128)S(1)}, f32[16,768]{1,0:T(8,128)}, u32[]{:S(2)}) copy-start(f32[16,768]{1,0:T(8,128)} %get-tuple-element.29) | copy-start | bytes 147460

commit v2 on v1

v2 whole, which is shorter than its diff:
```python
import jax
import jax.numpy as jnp
from jax import lax
from jax.experimental import pallas as pl
from jax.experimental.pallas import tpu as pltpu
from jax.sharding import Mesh
from jax.sharding import PartitionSpec as P

SP = ("sp_0", "sp_1", "sp_2")
MESH = pl.DeviceIdType.MESH
F32, BF16 = jnp.float32, jnp.bfloat16

norm_eps = 1e-05
LANES = 128
HALO = 32
AUX = 40
NX = NY = 4
NZ = 8
PLANE = NX * NY
VMEM_LIMIT = 32 * 1024 * 1024


def sigmoid(v):
    return 0.5 + 0.5 * jnp.tanh(0.5 * v)


def kernel(
    value_h, gate_h, out_h, taps_h, gain_h, shift_h, weight_h, og_h,
    gv_v, gg_v, gtaps_o, ggain_o, gshift_o, gproj_o,
    value_v, gate_v, out_v, taps_v, gain_v, shift_v, weight_v, og_v, in_sem,
    st_a, st_b, cen_b, inv_b, sum_b, dot_b, act_v, fac_v, sc_v, hg, gt, tapsf,
    gx, r1x, r2x, r3x, mx, hx, s1x, s2x, s3x, m2x, ex, zx,
    gy, r1y, r2y, r3y, my, hy, s1y, s2y, s3y, m2y, ey, zy,
    gz, rlz, rsz, mlz, msz, hz, s1z, s2z, s3z, m2z, ez, xz,
    red, red_r, zred, ag,
    st_sem, halo_sem, rs_send, rs_recv, z_send, z_recv, ar_send, ar_recv,
):
    rows, chans = value_v.shape
    groups = chans // LANES
    taps_n = taps_v.shape[0]
    reach = taps_n - 1
    chan_total = 2.0 * chans
    z, y, x = (lax.axis_index(a) for a in SP)
    core = lax.axis_index("tp")
    place = (z * NY + y) * NX + x
    last = NZ * PLANE
    blocks = rows // LANES

    def at_place(s):
        return {"sp_0": s // PLANE, "sp_1": lax.rem(s // NX, NY), "sp_2": lax.rem(s, NX)}

    nxt = at_place(lax.rem(place + 1, last))
    prv = at_place(lax.rem(place + last - 1, last))
    other = {"tp": 1 - core}

    def load(i, src, dst):
        c = pltpu.make_async_copy(src, dst, in_sem.at[i])
        c.start()
        return c

    sent = []

    def send(src, dst, ss, rs, dev):
        c = pltpu.make_async_remote_copy(
            src_ref=src, dst_ref=dst, send_sem=ss, recv_sem=rs, device_id=dev, device_id_type=MESH
        )
        c.start()
        sent.append(c)
        return c

    c_out = load(0, out_h, out_v)
    c_gain = load(1, gain_h, gain_v)
    c_shift = load(2, shift_h, shift_v)
    c_taps = load(3, taps_h, taps_v)
    c_gate = load(4, gate_h, gate_v)
    c_value = load(5, value_h, value_v)

    barrier = pltpu.get_barrier_semaphore()
    p_me = y * NX + x
    plane_dev = []
    plane_pos = []
    for k in range(1, PLANE):
        p = lax.rem(p_me + k, PLANE)
        plane_pos.append(p)
        plane_dev.append({"sp_1": p // NX, "sp_2": lax.rem(p, NX)})
    z_pos = [lax.rem(z + k, NZ) for k in range(1, NZ)]
    z_dev = [{"sp_0": p} for p in z_pos]
    x_pos = [lax.rem(x + k, NX) for k in range(1, NX)]
    x_dev = [{"sp_2": p} for p in x_pos]
    partners = [other, nxt, prv] + plane_dev + z_dev
    for dev in partners:
        pl.semaphore_signal(barrier, inc=1, device_id=dev, device_id_type=MESH)

    c_out.wait()
    c_og = load(6, og_h, og_v)

    def cols(g):
        return slice(g * LANES, (g + 1) * LANES)

    def blk(i):
        return slice(i * LANES, (i + 1) * LANES)

    eye = lax.broadcasted_iota(jnp.int32, (LANES, LANES), 0) == lax.broadcasted_iota(
        jnp.int32, (LANES, LANES), 1
    )
    for i in range(blocks):
        part = out_v[blk(i), cols(0)].astype(F32)
        for g in range(1, groups):
            part = part + out_v[blk(i), cols(g)].astype(F32)
        s = jnp.sum(part, axis=1, keepdims=True)
        m = s * (1.0 / chans)
        d = out_v[blk(i), cols(0)].astype(F32) - m
        sq = d * d
        for g in range(1, groups):
            d = out_v[blk(i), cols(g)].astype(F32) - m
            sq = sq + d * d
        st_a[0, i : i + 1, :] = jnp.sum(jnp.where(eye, s, 0.0), axis=0, keepdims=True)
        st_a[0, blocks + i : blocks + i + 1, :] = jnp.sum(sq.T, axis=0, keepdims=True)

    pl.semaphore_wait(barrier, len(partners))
    c_st1 = send(st_a.at[0], st_b.at[0], st_sem.at[0], st_sem.at[1], other)

    SB = 64
    c_gate.wait()
    c_value.wait()
    c_weight = load(7, weight_h, weight_v)

    @pl.loop(0, rows // SB)
    def _(i):
        rs = pl.ds(i * SB, SB)
        for g in range(groups):
            gated = value_v[rs, cols(g)].astype(F32) * sigmoid(gate_v[rs, cols(g)].astype(F32))
            gt[g, pl.ds(HALO + i * SB, SB), :] = gated.astype(BF16).astype(F32)

    c_gain.wait()
    c_shift.wait()
    c_taps.wait()
    for g in range(groups):
        tapsf[g, 0:taps_n, :] = taps_v[:, cols(g)].astype(F32)
    c_halo = send(
        gt.at[:, pl.ds(rows, HALO), :], gt.at[:, pl.ds(0, HALO), :],
        halo_sem.at[0], halo_sem.at[1], nxt,
    )
    c_st1.wait_recv()

    def spread(dst, src):
        for i in range(blocks):
            dst[blk(i), :] = jnp.broadcast_to(src[i : i + 1, :], (LANES, LANES)).T

    own, peer = st_a[0], st_b[0]
    s0, m0 = own[0:blocks], own[blocks : 2 * blocks]
    s1, m1 = peer[0:blocks], peer[blocks : 2 * blocks]
    ds = s0 - s1
    var = (m0 + m1 + ds * ds * (1.0 / chan_total)) * (1.0 / chan_total)
    spread(cen_b, (s0 + s1) * (1.0 / chan_total))
    spread(inv_b, lax.rsqrt(var + norm_eps))

    @pl.loop(0, rows // SB)
    def _(i):
        rs = pl.ds(i * SB, SB)
        cen, inv = cen_b[rs, :], inv_b[rs, :]
        for g in range(groups):
            sh = (out_v[rs, cols(g)].astype(F32) - cen) * inv * gain_v[g : g + 1, :] + shift_v[g : g + 1, :]
            sg = sigmoid(sh)
            act_v[rs, cols(g)] = (sh * sg).astype(BF16)
            fac_v[rs, cols(g)] = sg * (1.0 + sh * (1.0 - sg))

    c_og.wait()
    zb = PLANE * 16
    third = chans // 3
    HZ = NZ // 2

    def partial(zz, hf, zq):
        lhs = og_v[:, pl.ds(pl.multiple_of(zz * zb, zb), zb)]
        part = lax.dot_general(
            lhs, act_v[...], (((0,), (0,)), ((), ())), preferred_element_type=F32
        ).astype(BF16)
        for yy in range(NY):
            for xx in range(NX):
                r0 = (yy * NX + xx) * 16
                gx[xx, hf, yy * 4 + zq] = part[r0 : r0 + 16, 0:third]
                gy[yy, hf, xx * 4 + zq] = part[r0 : r0 + 16, third : 2 * third]
                gz[zz, yy // 2, (yy % 2) * 4 + xx] = part[r0 : r0 + 16, 2 * third :]

    DIRS = (1, -1)

    def tiles_add(n, step, fn):
        @pl.loop(0, n // step)
        def _(j):
            fn(j, pl.ds(j * step, step))

    class Ring4:
        def __init__(self, g, r1, r2, r3, m, axis, pos, base):
            self.g, self.r1, self.r2, self.r3, self.m = g, r1, r2, r3, m
            self.axis, self.pos, self.base = axis, pos, base
            self.a, self.b, self.c = {}, {}, {}
            self.n = r1.shape[1]
            self.step = min(4, self.n)

        def go(self, h, src, dst, slot, d):
            k = self.base + 2 * slot + h
            return send(src, dst, rs_send.at[k], rs_recv.at[k], {self.axis: lax.rem(self.pos + 4 + d, 4)})

        def start(self, h):
            d = DIRS[h]
            self.a[h] = self.go(h, self.g.at[lax.rem(self.pos + 2, 4), h], self.r1.at[h], 0, d)
            self.c[h] = self.go(h, self.g.at[lax.rem(self.pos + 4 - d, 4), h], self.r3.at[h], 1, -d)

        def mid(self, h):
            d = DIRS[h]
            self.a[h].wait_recv()
            idx = lax.rem(self.pos + 4 + d, 4)

            def fn(j, t):
                self.m[h, t] = (self.r1[h, t].astype(F32) + self.g[idx, h, t].astype(F32)).astype(BF16)

            tiles_add(self.n, self.step, fn)
            self.b[h] = self.go(h, self.m.at[h], self.r2.at[h], 2, d)

        def end(self, h, write):
            self.c[h].wait_recv()
            self.b[h].wait_recv()

            def fn(j, t):
                v = self.r2[h, t].astype(F32) + self.r3[h, t].astype(F32) + self.g[self.pos, h, t].astype(F32)
                write(h, j, v.astype(BF16))

            tiles_add(self.n, self.step, fn)

    class Ring8:
        def __init__(self):
            self.l, self.s = {}, {}

        def g(self, h, k):
            return gz.at[lax.rem(z + 16 + k * DIRS[h], NZ), h]

        def go(self, h, src, dst, slot, d):
            k = 24 + 2 * slot + h
            return send(src, dst, rs_send.at[k], rs_recv.at[k], {"sp_0": lax.rem(z + NZ + d, NZ)})

        def start(self, h):
            d = DIRS[h]
            self.l[h] = self.go(h, self.g(h, 4), rlz.at[h, 0], 0, d)
            self.s[h] = self.go(h, self.g(h, -3), rsz.at[h, 0], 4, -d)

        def add(self, h, r, q, m, k):
            own = self.g(h, k)

            def fn(j, t):
                m[h, q, t] = (r[h, q, t].astype(F32) + own[t].astype(F32)).astype(BF16)

            tiles_add(8, 4, fn)

        def long(self, h, r):
            self.l[h].wait_recv()
            self.add(h, rlz, r - 1, mlz, 4 - r)
            self.l[h] = self.go(h, mlz.at[h, r - 1], rlz.at[h, r], r, DIRS[h])

        def short(self, h, r):
            self.s[h].wait_recv()
            self.add(h, rsz, r - 1, msz, r - 3)
            self.s[h] = self.go(h, msz.at[h, r - 1], rsz.at[h, r], 4 + r, -DIRS[h])

        def end(self, h):
            self.l[h].wait_recv()
            self.s[h].wait_recv()
            for yl in range(2):
                t = slice(4 * yl, 4 * yl + 4)
                v = rlz[h, 3, t].astype(F32) + rsz[h, 2, t].astype(F32) + gz[z, h, t].astype(F32)
                v = v.astype(BF16)
                hz[2 * h + yl, 0] = v[0:2]
                hz[2 * h + yl, 1] = v[2:4]

    rx = Ring4(gx, r1x, r2x, r3x, mx, "sp_2", x, 0)
    ry = Ring4(gy, r1y, r2y, r3y, my, "sp_1", y, 6)
    rz = Ring8()
    qx = Ring4(hx, s1x, s2x, s3x, m2x, "sp_1", y, 12)
    qy = Ring4(hy, s1y, s2y, s3y, m2y, "sp_2", x, 18)
    qz = Ring4(hz, s1z, s2z, s3z, m2z, "sp_1", y, 38)

    for hf in range(2):

        @pl.loop(0, HZ)
        def _(zq, hf=hf):
            partial(zq + hf * HZ, hf, zq)

        rx.start(hf)
        ry.start(hf)
    for hf in range(2):
        rz.start(hf)

    c_weight.wait()
    NB = 256

    @pl.loop(0, chans // NB)
    def _(n):
        cs = pl.ds(pl.multiple_of(n * NB, NB), NB)
        sc_v[:, cs] = jnp.dot(og_v[...], weight_v[:, cs], preferred_element_type=F32)

    zero = jnp.zeros((8, LANES), F32)

    def norm_pass(i, carry):
        rs = pl.ds(i * SB, SB)
        cen, inv = cen_b[rs, :], inv_b[rs, :]
        r_sum = jnp.zeros((SB, LANES), F32)
        r_dot = jnp.zeros((SB, LANES), F32)
        new = []
        for g in range(groups):
            n = sc_v[rs, cols(g)] * fac_v[rs, cols(g)]
            xc = (out_v[rs, cols(g)].astype(F32) - cen) * inv
            nx = n * xc
            new.append(carry[2 * g] + jnp.sum(nx.reshape(SB // 8, 8, LANES), axis=0))
            new.append(carry[2 * g + 1] + jnp.sum(n.reshape(SB // 8, 8, LANES), axis=0))
            sc = n * gain_v[g : g + 1, :]
            r_sum = r_sum + sc
            r_dot = r_dot + sc * xc
            sc_v[rs, cols(g)] = sc
        sum_b[rs, :] = r_sum
        dot_b[rs, :] = r_dot
        return tuple(new)

    sums = lax.fori_loop(0, rows // SB, norm_pass, (zero,) * (2 * groups))
    for i in range(blocks):
        st_a[1, i : i + 1, :] = jnp.sum(sum_b[blk(i), :].T, axis=0, keepdims=True)
        st_a[1, blocks + i : blocks + i + 1, :] = jnp.sum(dot_b[blk(i), :].T, axis=0, keepdims=True)
    c_st2 = send(st_a.at[1], st_b.at[1], st_sem.at[2], st_sem.at[3], other)

    def put_row(g, j, row):
        red[(g * AUX + j) // 8, j % 8 : j % 8 + 1, :] = row

    for g in range(groups):
        put_row(g, taps_n, jnp.sum(sums[2 * g], axis=0, keepdims=True))
        put_row(g, taps_n + 1, jnp.sum(sums[2 * g + 1], axis=0, keepdims=True))
        for j in range(taps_n + 2, AUX):
            put_row(g, j, jnp.zeros((1, LANES), F32))
    for t in range(groups * AUX // 8, red.shape[0]):
        red[t] = zero

    for h in range(2):
        rx.mid(h) if h == 0 else None
        ry.mid(h) if h == 0 else None
        rz.long(h, 1)
    c_st2.wait_recv()

    both = (st_a[1] + st_b[1]) * (1.0 / chan_total)
    spread(sum_b, both[0:blocks])
    spread(dot_b, both[blocks : 2 * blocks])

    @pl.loop(0, rows // SB)
    def _(i):
        rs = pl.ds(i * SB, SB)
        cen, inv = cen_b[rs, :], inv_b[rs, :]
        gs, gd = sum_b[rs, :], dot_b[rs, :]
        for g in range(groups):
            xc = (out_v[rs, cols(g)].astype(F32) - cen) * inv
            hg[g, rs, :] = inv * (sc_v[rs, cols(g)] - gs - xc * gd)

    c_back = send(
        hg.at[:, pl.ds(0, HALO), :], hg.at[:, pl.ds(rows, HALO), :],
        halo_sem.at[2], halo_sem.at[3], prv,
    )
    c_halo.wait_recv()

    @pl.when(place == 0)
    def _():
        gt[:, 0:HALO, :] = jnp.zeros((groups, HALO, LANES), F32)

    UB = 8

    def taps_part(lo, hi):
        @pl.loop(lo, hi)
        def _(g):
            def step(t, acc):
                base = pl.multiple_of(t * (8 * UB), 8 * UB)
                hs = [hg[g, pl.ds(base + 8 * b, 8), :] for b in range(UB)]
                acc = list(acc)
                for o in range(taps_n + 8 * (UB - 1)):
                    v = gt[g, pl.ds(base + (HALO - reach + o), 8), :]
                    for b in range(UB):
                        if 0 <= o - 8 * b < taps_n:
                            acc[o - 8 * b] = acc[o - 8 * b] + hs[b] * v
                return tuple(acc)

            acc = lax.fori_loop(0, rows // (8 * UB), step, (zero,) * taps_n)
            for j in range(taps_n):
                red[g * (AUX // 8) + j // 8, j % 8 : j % 8 + 1, :] = jnp.sum(
                    acc[j], axis=0, keepdims=True
                )

    TB = 8 * UB

    def gated_part(lo, hi):
        @pl.loop(lo, hi)
        def _(g):
            weights = [jnp.broadcast_to(tapsf[g, j : j + 1, :], (8, LANES)) for j in range(taps_n)]
            cs = pl.ds(pl.multiple_of(g * LANES, LANES), LANES)

            @pl.loop(0, rows // TB)
            def _(t):
                base = pl.multiple_of(t * TB, TB)
                parts = [None] * UB
                for o in range(taps_n + TB - 8):
                    v = hg[g, pl.ds(base + o, 8), :]
                    for b in range(UB):
                        j = 8 * b + reach - o
                        if 0 <= j < taps_n:
                            term = weights[j] * v
                            parts[b] = term if parts[b] is None else parts[b] + term
                gg = jnp.concatenate(parts, axis=0)
                rs = pl.ds(base, TB)
                sg = sigmoid(gate_v[rs, cs].astype(F32))
                val = value_v[rs, cs].astype(F32)
                gs = gg * sg
                gv_v[rs, cs] = gs.astype(BF16)
                gg_v[rs, cs] = (gs * val * (1.0 - sg)).astype(BF16)

    taps_part(0, 2)
    for h in range(2):
        rz.short(h, 1)
    rx.mid(1)
    ry.mid(1)
    taps_part(2, 4)
    for h in range(2):
        rz.long(h, 2)
    taps_part(4, groups)

    ar_a = []
    for k in range(1, PLANE):
        ar_a.append(send(
            red.at[pl.ds(2 * plane_pos[k - 1], 2)], red_r.at[k - 1],
            ar_send.at[k - 1], ar_recv.at[k - 1], plane_dev[k - 1],
        ))
    for h in range(2):
        rz.short(h, 2)
    c_back.wait_recv()

    @pl.when(place == last - 1)
    def _():
        hg[:, rows : rows + HALO, :] = jnp.zeros((groups, HALO, LANES), F32)

    gated_part(0, 1)
    for h in range(2):
        rz.long(h, 3)

    def to_hx(h, j, v):
        hx[j, h] = v

    def to_hy(h, j, v):
        hy[j, h] = v

    gated_part(1, 2)
    for h in range(2):
        rx.end(h, to_hx)
        qx.start(h) if h else None
        ry.end(h, to_hy)
    qx.start(0)
    qy.start(1)
    qy.start(0)

    gated_part(2, 4)
    for c in ar_a:
        c.wait_recv()
    mine = red[pl.ds(2 * p_me, 2)]
    for k in range(PLANE - 1):
        mine = mine + red_r[k]
    zred[z] = mine
    ar_b = []
    for k in range(1, NZ):
        ar_b.append(send(
            zred.at[z], zred.at[z], ar_send.at[PLANE + k], ar_recv.at[PLANE + k], z_dev[k - 1],
        ))

    gated_part(4, 5)
    for h in range(2):
        qx.mid(h)
        qy.mid(h)
    gated_part(5, groups)
    for h in range(2):
        rz.end(h)
    for h in range(2):
        qz.start(h)

    def to_e(e, n):
        def write(h, j, v):
            e[h * n : (h + 1) * n] = v

        return write

    zs = []
    for c, (q, e, zr) in enumerate(((qx, ex, zx), (qy, ey, zy))):
        for h in range(2):
            q.end(h, to_e(e, HZ))
        for k in range(1, NZ):
            zs.append(send(
                e.at[z_pos[k - 1]], zr.at[k - 1],
                z_send.at[c * NZ + k], z_recv.at[c * NZ + k], z_dev[k - 1],
            ))

    for c in ar_b:
        c.wait_recv()
    total = zred[0]
    for k in range(1, NZ):
        total = total + zred[k]
    ag[pl.ds(2 * p_me, 2)] = total
    ar_c = []
    for k in range(1, PLANE):
        ar_c.append(send(
            ag.at[pl.ds(2 * p_me, 2)], ag.at[pl.ds(2 * p_me, 2)],
            ar_send.at[PLANE + NZ + k], ar_recv.at[PLANE + NZ + k], plane_dev[k - 1],
        ))

    for h in range(2):
        qz.mid(h)
    for h in range(2):
        qz.end(h, to_e(ez, 2))
    xs = []
    for k in range(1, NX):
        xs.append(send(
            ez.at[x_pos[k - 1]], xz.at[k - 1],
            z_send.at[2 * NZ + k], z_recv.at[2 * NZ + k], x_dev[k - 1],
        ))

    for c in ar_c:
        c.wait_recv()
    for g in range(groups):
        for u in range(AUX // 8):
            tile = ag[g * (AUX // 8) + u]
            if u < taps_n // 8:
                gtaps_o[u * 8 : u * 8 + 8, cols(g)] = tile
            elif u == taps_n // 8:
                gtaps_o[u * 8 : taps_n, cols(g)] = tile[0 : taps_n - u * 8]
        for j, o in ((taps_n, ggain_o), (taps_n + 1, gshift_o)):
            o[g : g + 1, :] = ag[(g * AUX + j) // 8, j % 8 : j % 8 + 1, :]

    def last_sum(c, e, pos, r, copies):
        for k in copies:
            k.wait_recv()
        t = e[pos].astype(F32)
        for k in range(r.shape[0]):
            t = t + r[k].astype(F32)
        gproj_o[:, c * third : (c + 1) * third] = t

    last_sum(0, ex, z, zx, zs[: NZ - 1])
    last_sum(1, ey, z, zy, zs[NZ - 1 :])
    last_sum(2, ez, x, xz, xs)

    for c in sent:
        c.wait_send()


def put_kernel(*refs):
    n = len(refs) // 2
    sem = refs[-1]
    copies = [pltpu.make_async_copy(refs[i], refs[n + i], sem.at[i]) for i in range(n)]
    for c in copies:
        c.start()
    for c in copies:
        c.wait()


def local(conv_value, conv_gate, conv_out, conv_taps, norm_gain, norm_shift, proj_weight, out_grad):
    rows, chans = conv_value.shape
    taps_n = conv_taps.shape[0]
    d_model = proj_weight.shape[0]
    groups = chans // LANES
    third = chans // 3
    hbm_s = pl.BlockSpec(memory_space=pltpu.HBM)
    vm_s = pl.BlockSpec(memory_space=pltpu.VMEM)
    V = pltpu.VMEM
    DMA = pltpu.SemaphoreType.DMA

    def color():
        unit, small = (2, 16, 16, third), (2, 4, 16, third)
        return [
            V((4, 2, 16, 16, third), BF16),
            V(unit, BF16), V(unit, BF16), V(unit, BF16), V(unit, BF16),
            V((4, 2, 4, 16, third), BF16),
            V(small, BF16), V(small, BF16), V(small, BF16), V(small, BF16),
            V((8, 16, third), BF16),
            V((7, 16, third), BF16),
        ]

    tiny = (2, 2, 16, third)
    scratch = [
        V((rows, chans), BF16), V((rows, chans), BF16), V((rows, chans), BF16),
        V((taps_n, chans), BF16), V((groups, LANES), F32), V((groups, LANES), F32),
        V((d_model, chans), BF16), V((rows, d_model), BF16), DMA((8,)),
        V((2, 8, LANES), F32), V((2, 8, LANES), F32),
        *[V((rows, LANES), F32)] * 4,
        V((rows, chans), BF16), V((rows, chans), F32), V((rows, chans), F32),
        V((groups, rows + HALO, LANES), F32), V((groups, rows + HALO, LANES), F32),
        V((groups, 32, LANES), F32),
        *color(), *color(),
        V((8, 2, 8, 16, third), BF16),
        V((2, 4, 8, 16, third), BF16), V((2, 3, 8, 16, third), BF16),
        V((2, 3, 8, 16, third), BF16), V((2, 2, 8, 16, third), BF16),
        V((4, 2, 2, 16, third), BF16),
        V(tiny, BF16), V(tiny, BF16), V(tiny, BF16), V(tiny, BF16),
        V((4, 16, third), BF16), V((3, 16, third), BF16),
        V((32, 8, LANES), F32), V((PLANE - 1, 2, 8, LANES), F32), V((NZ, 2, 8, LANES), F32),
        V((32, 8, LANES), F32),
        DMA((4,)), DMA((4,)), DMA((44,)), DMA((44,)), DMA((2 * NZ + NX,)), DMA((2 * NZ + NX,)),
        DMA((2 * PLANE + NZ,)), DMA((2 * PLANE + NZ,)),
    ]
    S = jax.ShapeDtypeStruct
    shapes = (
        S((rows, chans), BF16), S((rows, chans), BF16), S((taps_n, chans), F32),
        S((groups, LANES), F32), S((groups, LANES), F32), S((16, chans), F32),
    )
    held = pl.pallas_call(
        kernel,
        name="conv_backward",
        out_shape=shapes,
        in_specs=[hbm_s] * 8,
        out_specs=(vm_s,) * 6,
        scratch_shapes=scratch,
        compiler_params=pltpu.CompilerParams(
            collective_id=0, has_side_effects=True, vmem_limit_bytes=VMEM_LIMIT
        ),
    )(*(
        pltpu.with_memory_space_constraint(a, pltpu.HBM)
        for a in (
            conv_value, conv_gate, conv_out, conv_taps,
            norm_gain.reshape(groups, LANES), norm_shift.reshape(groups, LANES), proj_weight, out_grad,
        )
    ))
    gv, gg, gtaps, ggain, gshift, gproj = pl.pallas_call(
        put_kernel,
        name="put_outputs",
        out_shape=shapes,
        in_specs=[vm_s] * len(shapes),
        out_specs=(hbm_s,) * len(shapes),
        scratch_shapes=[DMA((len(shapes),))],
        compiler_params=pltpu.CompilerParams(vmem_limit_bytes=1024 * 1024),
    )(*held)
    return gv, gg, gtaps, ggain.reshape(chans), gshift.reshape(chans), gproj


def solution(mesh):
    split = Mesh(mesh.devices.reshape(8, 4, 4, mesh.shape["tp"]), (*SP, "tp"))
    placed = (
        P(SP, "tp"), P(SP, "tp"), P(SP, "tp"), P(None, "tp"),
        P("tp"), P("tp"), P(None, "tp"), P(SP, None),
    )
    return jax.shard_map(
        local,
        mesh=split,
        in_specs=placed,
        out_specs=(P(SP, "tp"), P(SP, "tp"), P(None, "tp"), P("tp"), P("tp"), P(SP, "tp")),
        check_vma=False,
    )
```

time: 66.9 us -> 48.9 us (0.73)
  the two profiles are of different devices: /device:TPU:6 before, /device:TPU:2 now
where the time goes in v2:
time: 48.9 us; the launch traced here: 48.8 us
  Pallas kernels  48.2 us (99%)
  between operations  0.64 us (1%)
    pallas_call x1, Pallas kernels, local(): pl.pallas_call(kernel, name='conv_backward', out_shape=shapes, in_specs=[...  47 us
    pallas_call x1, Pallas kernels, local(): pl.pallas_call(put_kernel, name='put_outputs', out_shape=shapes, in_specs...  1.23 us

profile of v2, /device:TPU:2, one launch (start us, length us, event | category | flops | bytes accessed | tf_op | source)
XLA Modules:
  0.0 48.8 jit_solution(11026304604815246060)
XLA Ops:
  0.6 47.0 %conv_backward.1 = (bf16[512,768]{1,0:T(8,128)(2,1)S(1)}, bf16[512,768]{1,0:T(8,128)(2,1)S(1)}, f32[31,768]{1,0:T(8,128)S(1)}, f32[6,128]{1,0:T(8,128)S(1)}, f32...) custom-call(bf16[512,768]{1,0:T(8,128)(2,1)} %value_h.1, bf16[512,768]{1,0:T(8,128)(2,1)} %gate_h.1, bf16[512,768]{1,0:T(8,128)(2,1)} %out_h.1, ...), custom_call_target="tpu_custom_call" | custom-call | tf_op jit(solution)/shard_map/conv_backward/pallas_call | solution.py:610
  47.6 1.2 %put_outputs.1 = (bf16[512,768]{1,0:T(8,128)(2,1)}, bf16[512,768]{1,0:T(8,128)(2,1)}, f32[31,768]{1,0:T(8,128)}, f32[6,128]{1,0:T(8,128)}, f32[6,128]{1,0:T(8,128)}, /*index=5*/f32[16,768]{1,0:T(8,128)}) custom-call(bf16[512,768]{1,0:T(8,128)(2,1)S(1)} %get-tuple-element.18.refs_0_, bf16[512,768]{1,0:T(8,128)(2,1)S(1)} %get-tuple-element.19.refs_1_, ...), custom_call_target="tpu_custom_call" | custom-call | tf_op jit(solution)/shard_map/put_outputs/pallas_call | solution.py:627

commit v3 on v2

--- a/solution.py
+++ b/solution.py
@@ -29,9 +29,9 @@
     gv_v, gg_v, gtaps_o, ggain_o, gshift_o, gproj_o,
     value_v, gate_v, out_v, taps_v, gain_v, shift_v, weight_v, og_v, in_sem,
     st_a, st_b, cen_b, inv_b, sum_b, dot_b, act_v, fac_v, sc_v, hg, gt, tapsf,
-    gx, r1x, r2x, r3x, mx, hx, s1x, s2x, s3x, m2x, ex, zx,
-    gy, r1y, r2y, r3y, my, hy, s1y, s2y, s3y, m2y, ey, zy,
-    gz, rlz, rsz, mlz, msz, hz, s1z, s2z, s3z, m2z, ez, xz,
+    gx, r_x, mx, hx, s_x, m2x, ex, zx,
+    gy, r_y, my, hy, s_y, m2y, ey, zy,
+    gz, r_z, mz, hz, pz,
     red, red_r, zred, ag,
     st_sem, halo_sem, rs_send, rs_recv, z_send, z_recv, ar_send, ar_recv,
 ):
@@ -58,15 +58,17 @@
         c.start()
         return c
 
-    sent = []
-
     def send(src, dst, ss, rs, dev):
         c = pltpu.make_async_remote_copy(
             src_ref=src, dst_ref=dst, send_sem=ss, recv_sem=rs, device_id=dev, device_id_type=MESH
         )
         c.start()
-        sent.append(c)
         return c
+
+    def total(ref, ss, rs):
+        return pltpu.make_async_remote_copy(
+            src_ref=ref, dst_ref=ref, send_sem=ss, recv_sem=rs, device_id=other, device_id_type=MESH
+        )
 
     c_out = load(0, out_h, out_v)
     c_gain = load(1, gain_h, gain_v)
@@ -85,8 +87,6 @@
         plane_dev.append({"sp_1": p // NX, "sp_2": lax.rem(p, NX)})
     z_pos = [lax.rem(z + k, NZ) for k in range(1, NZ)]
     z_dev = [{"sp_0": p} for p in z_pos]
-    x_pos = [lax.rem(x + k, NX) for k in range(1, NX)]
-    x_dev = [{"sp_2": p} for p in x_pos]
     partners = [other, nxt, prv] + plane_dev + z_dev
     for dev in partners:
         pl.semaphore_signal(barrier, inc=1, device_id=dev, device_id_type=MESH)
@@ -170,17 +170,21 @@
     third = chans // 3
     HZ = NZ // 2
 
-    def partial(zz, hf, zq):
-        lhs = og_v[:, pl.ds(pl.multiple_of(zz * zb, zb), zb)]
+    ZM = 4
+
+    def partial(hf):
+        m = ZM * zb
+        lhs = og_v[:, hf * m : (hf + 1) * m]
         part = lax.dot_general(
             lhs, act_v[...], (((0,), (0,)), ((), ())), preferred_element_type=F32
         ).astype(BF16)
-        for yy in range(NY):
-            for xx in range(NX):
-                r0 = (yy * NX + xx) * 16
-                gx[xx, hf, yy * 4 + zq] = part[r0 : r0 + 16, 0:third]
-                gy[yy, hf, xx * 4 + zq] = part[r0 : r0 + 16, third : 2 * third]
-                gz[zz, yy // 2, (yy % 2) * 4 + xx] = part[r0 : r0 + 16, 2 * third :]
+        for zq in range(ZM):
+            for yy in range(NY):
+                for xx in range(NX):
+                    r0 = zq * zb + (yy * NX + xx) * 16
+                    gx[xx, hf, yy * 4 + zq] = part[r0 : r0 + 16, 0:third]
+                    gy[yy, hf, xx * 4 + zq] = part[r0 : r0 + 16, third : 2 * third]
+                    gz[hf * ZM + zq, yy // 2, (yy % 2) * 4 + xx] = part[r0 : r0 + 16, 2 * third :]
 
     DIRS = (1, -1)
 
@@ -190,100 +194,105 @@
             fn(j, pl.ds(j * step, step))
 
     class Ring4:
-        def __init__(self, g, r1, r2, r3, m, axis, pos, base):
-            self.g, self.r1, self.r2, self.r3, self.m = g, r1, r2, r3, m
-            self.axis, self.pos, self.base = axis, pos, base
-            self.a, self.b, self.c = {}, {}, {}
-            self.n = r1.shape[1]
+        def __init__(self, g, r, m, axis, pos, base, sem):
+            self.g, self.r, self.m = g, r, m
+            self.axis, self.pos, self.base, self.sem = axis, pos, base, sem
+            self.c = {}
+            self.n = r.shape[2]
             self.step = min(4, self.n)
 
-        def go(self, h, src, dst, slot, d):
-            k = self.base + 2 * slot + h
-            return send(src, dst, rs_send.at[k], rs_recv.at[k], {self.axis: lax.rem(self.pos + 4 + d, 4)})
+        def go(self, h, src, slot, d):
+            self.c[slot, h] = send(
+                src, self.r.at[slot, h], rs_send.at[self.sem], rs_recv.at[self.base + 2 * slot + h],
+                {self.axis: lax.rem(self.pos + 4 + d, 4)},
+            )
 
         def start(self, h):
             d = DIRS[h]
-            self.a[h] = self.go(h, self.g.at[lax.rem(self.pos + 2, 4), h], self.r1.at[h], 0, d)
-            self.c[h] = self.go(h, self.g.at[lax.rem(self.pos + 4 - d, 4), h], self.r3.at[h], 1, -d)
+            self.go(h, self.g.at[lax.rem(self.pos + 2, 4), h], 0, d)
+            self.go(h, self.g.at[lax.rem(self.pos + 4 - d, 4), h], 1, -d)
 
         def mid(self, h):
             d = DIRS[h]
-            self.a[h].wait_recv()
+            self.c[0, h].wait_recv()
             idx = lax.rem(self.pos + 4 + d, 4)
 
             def fn(j, t):
-                self.m[h, t] = (self.r1[h, t].astype(F32) + self.g[idx, h, t].astype(F32)).astype(BF16)
+                self.m[h, t] = (self.r[0, h, t].astype(F32) + self.g[idx, h, t].astype(F32)).astype(BF16)
 
             tiles_add(self.n, self.step, fn)
-            self.b[h] = self.go(h, self.m.at[h], self.r2.at[h], 2, d)
+            self.go(h, self.m.at[h], 2, d)
 
         def end(self, h, write):
-            self.c[h].wait_recv()
-            self.b[h].wait_recv()
+            self.c[1, h].wait_recv()
+            self.c[2, h].wait_recv()
 
             def fn(j, t):
-                v = self.r2[h, t].astype(F32) + self.r3[h, t].astype(F32) + self.g[self.pos, h, t].astype(F32)
+                v = self.r[1, h, t].astype(F32) + self.r[2, h, t].astype(F32) + self.g[self.pos, h, t].astype(F32)
                 write(h, j, v.astype(BF16))
 
             tiles_add(self.n, self.step, fn)
 
+        def drain(self):
+            total(self.r, rs_send.at[self.sem], rs_recv.at[self.base]).wait_send()
+
     class Ring8:
-        def __init__(self):
-            self.l, self.s = {}, {}
+        def __init__(self, base, sem):
+            self.base, self.sem = base, sem
+            self.c = {}
 
         def g(self, h, k):
             return gz.at[lax.rem(z + 16 + k * DIRS[h], NZ), h]
 
-        def go(self, h, src, dst, slot, d):
-            k = 24 + 2 * slot + h
-            return send(src, dst, rs_send.at[k], rs_recv.at[k], {"sp_0": lax.rem(z + NZ + d, NZ)})
+        def go(self, h, src, slot, d):
+            self.c[slot, h] = send(
+                src, r_z.at[slot, h], rs_send.at[self.sem], rs_recv.at[self.base + 2 * slot + h],
+                {"sp_0": lax.rem(z + NZ + d, NZ)},
+            )
 
         def start(self, h):
             d = DIRS[h]
-            self.l[h] = self.go(h, self.g(h, 4), rlz.at[h, 0], 0, d)
-            self.s[h] = self.go(h, self.g(h, -3), rsz.at[h, 0], 4, -d)
-
-        def add(self, h, r, q, m, k):
+            self.go(h, self.g(h, 4), 0, d)
+            self.go(h, self.g(h, -3), 4, -d)
+
+        def hop(self, h, slot, k, d):
+            self.c[slot, h].wait_recv()
             own = self.g(h, k)
+            q = slot if slot < 4 else slot - 1
 
             def fn(j, t):
-                m[h, q, t] = (r[h, q, t].astype(F32) + own[t].astype(F32)).astype(BF16)
+                mz[q, h, t] = (r_z[slot, h, t].astype(F32) + own[t].astype(F32)).astype(BF16)
 
             tiles_add(8, 4, fn)
+            self.go(h, mz.at[q, h], slot + 1, d)
 
         def long(self, h, r):
-            self.l[h].wait_recv()
-            self.add(h, rlz, r - 1, mlz, 4 - r)
-            self.l[h] = self.go(h, mlz.at[h, r - 1], rlz.at[h, r], r, DIRS[h])
+            self.hop(h, r - 1, 4 - r, DIRS[h])
 
         def short(self, h, r):
-            self.s[h].wait_recv()
-            self.add(h, rsz, r - 1, msz, r - 3)
-            self.s[h] = self.go(h, msz.at[h, r - 1], rsz.at[h, r], 4 + r, -DIRS[h])
+            self.hop(h, 3 + r, r - 3, -DIRS[h])
 
         def end(self, h):
-            self.l[h].wait_recv()
-            self.s[h].wait_recv()
-            for yl in range(2):
-                t = slice(4 * yl, 4 * yl + 4)
-                v = rlz[h, 3, t].astype(F32) + rsz[h, 2, t].astype(F32) + gz[z, h, t].astype(F32)
-                v = v.astype(BF16)
-                hz[2 * h + yl, 0] = v[0:2]
-                hz[2 * h + yl, 1] = v[2:4]
-
-    rx = Ring4(gx, r1x, r2x, r3x, mx, "sp_2", x, 0)
-    ry = Ring4(gy, r1y, r2y, r3y, my, "sp_1", y, 6)
-    rz = Ring8()
-    qx = Ring4(hx, s1x, s2x, s3x, m2x, "sp_1", y, 12)
-    qy = Ring4(hy, s1y, s2y, s3y, m2y, "sp_2", x, 18)
-    qz = Ring4(hz, s1z, s2z, s3z, m2z, "sp_1", y, 38)
+            self.c[3, h].wait_recv()
+            self.c[6, h].wait_recv()
+
+            def fn(j, t):
+                v = r_z[3, h, t].astype(F32) + r_z[6, h, t].astype(F32) + gz[z, h, t].astype(F32)
+                hz[pl.ds(h * 8 + j * 4, 4)] = v.astype(BF16)
+
+            tiles_add(8, 4, fn)
+
+        def drain(self):
+            total(r_z, rs_send.at[self.sem], rs_recv.at[self.base]).wait_send()
+
+    rx = Ring4(gx, r_x, mx, "sp_2", x, 0, 0)
+    ry = Ring4(gy, r_y, my, "sp_1", y, 6, 1)
+    qx = Ring4(hx, s_x, m2x, "sp_1", y, 12, 2)
+    qy = Ring4(hy, s_y, m2y, "sp_2", x, 18, 3)
+    rz = Ring8(24, 4)
 
     for hf in range(2):
-
-        @pl.loop(0, HZ)
-        def _(zq, hf=hf):
-            partial(zq + hf * HZ, hf, zq)
-
+        partial(hf)
         rx.start(hf)
         ry.start(hf)
     for hf in range(2):
@@ -336,10 +345,6 @@
     for t in range(groups * AUX // 8, red.shape[0]):
         red[t] = zero
 
-    for h in range(2):
-        rx.mid(h) if h == 0 else None
-        ry.mid(h) if h == 0 else None
-        rz.long(h, 1)
     c_st2.wait_recv()
 
     both = (st_a[1] + st_b[1]) * (1.0 / chan_total)
@@ -359,6 +364,11 @@
         hg.at[:, pl.ds(0, HALO), :], hg.at[:, pl.ds(rows, HALO), :],
         halo_sem.at[2], halo_sem.at[3], prv,
     )
+    rx.mid(0)
+    ry.mid(0)
+    for h in range(2):
+        rz.long(h, 1)
+
     c_halo.wait_recv()
 
     @pl.when(place == 0)
@@ -414,24 +424,38 @@
                 gv_v[rs, cs] = gs.astype(BF16)
                 gg_v[rs, cs] = (gs * val * (1.0 - sg)).astype(BF16)
 
+    def to_hx(h, j, v):
+        hx[j, h] = v
+
+    def to_hy(h, j, v):
+        hy[j, h] = v
+
+    def to_e(e):
+        def write(h, j, v):
+            e[h * HZ : (h + 1) * HZ] = v
+
+        return write
+
+    def send_z(i, e, zr, h):
+        for p in range(h * HZ, (h + 1) * HZ):
+
+            @pl.when(z != p)
+            def _(p=p):
+                send(e.at[p], zr.at[z], z_send.at[i], z_recv.at[i], {"sp_0": p})
+
     taps_part(0, 2)
     for h in range(2):
         rz.short(h, 1)
     rx.mid(1)
     ry.mid(1)
-    taps_part(2, 4)
+    taps_part(2, groups)
+    for k in range(1, PLANE):
+        send(
+            red.at[pl.ds(2 * plane_pos[k - 1], 2)], red_r.at[k - 1],
+            ar_send.at[0], ar_recv.at[0], plane_dev[k - 1],
+        )
     for h in range(2):
         rz.long(h, 2)
-    taps_part(4, groups)
-
-    ar_a = []
-    for k in range(1, PLANE):
-        ar_a.append(send(
-            red.at[pl.ds(2 * plane_pos[k - 1], 2)], red_r.at[k - 1],
-            ar_send.at[k - 1], ar_recv.at[k - 1], plane_dev[k - 1],
-        ))
-    for h in range(2):
-        rz.short(h, 2)
     c_back.wait_recv()
 
     @pl.when(place == last - 1)
@@ -439,89 +463,66 @@
         hg[:, rows : rows + HALO, :] = jnp.zeros((groups, HALO, LANES), F32)
 
     gated_part(0, 1)
+    rx.end(0, to_hx)
+    qx.start(0)
+    ry.end(0, to_hy)
+    qy.start(0)
+    for h in range(2):
+        rz.short(h, 2)
+    gated_part(1, 2)
+    rx.end(1, to_hx)
+    qx.start(1)
+    ry.end(1, to_hy)
+    qy.start(1)
+    gated_part(2, 4)
     for h in range(2):
         rz.long(h, 3)
-
-    def to_hx(h, j, v):
-        hx[j, h] = v
-
-    def to_hy(h, j, v):
-        hy[j, h] = v
-
-    gated_part(1, 2)
-    for h in range(2):
-        rx.end(h, to_hx)
-        qx.start(h) if h else None
-        ry.end(h, to_hy)
-    qx.start(0)
-    qy.start(1)
-    qy.start(0)
-
-    gated_part(2, 4)
-    for c in ar_a:
-        c.wait_recv()
+    qx.mid(0)
+    qy.mid(0)
+    total(red_r, ar_send.at[0], ar_recv.at[0]).wait_recv()
     mine = red[pl.ds(2 * p_me, 2)]
     for k in range(PLANE - 1):
         mine = mine + red_r[k]
     zred[z] = mine
-    ar_b = []
     for k in range(1, NZ):
-        ar_b.append(send(
-            zred.at[z], zred.at[z], ar_send.at[PLANE + k], ar_recv.at[PLANE + k], z_dev[k - 1],
-        ))
-
+        send(zred.at[z], zred.at[z], ar_send.at[1], ar_recv.at[1], z_dev[k - 1])
     gated_part(4, 5)
-    for h in range(2):
-        qx.mid(h)
-        qy.mid(h)
+    qx.mid(1)
+    qy.mid(1)
     gated_part(5, groups)
+    qx.end(0, to_e(ex))
+    send_z(0, ex, zx, 0)
+    qy.end(0, to_e(ey))
+    send_z(1, ey, zy, 0)
     for h in range(2):
         rz.end(h)
-    for h in range(2):
-        qz.start(h)
-
-    def to_e(e, n):
-        def write(h, j, v):
-            e[h * n : (h + 1) * n] = v
-
-        return write
-
-    zs = []
-    for c, (q, e, zr) in enumerate(((qx, ex, zx), (qy, ey, zy))):
-        for h in range(2):
-            q.end(h, to_e(e, HZ))
-        for k in range(1, NZ):
-            zs.append(send(
-                e.at[z_pos[k - 1]], zr.at[k - 1],
-                z_send.at[c * NZ + k], z_recv.at[c * NZ + k], z_dev[k - 1],
-            ))
-
-    for c in ar_b:
-        c.wait_recv()
-    total = zred[0]
+    for k in range(1, PLANE):
+        send(
+            hz.at[plane_pos[k - 1]], pz.at[k - 1], z_send.at[2], z_recv.at[2], plane_dev[k - 1],
+        )
+    qx.end(1, to_e(ex))
+    send_z(0, ex, zx, 1)
+    qy.end(1, to_e(ey))
+    send_z(1, ey, zy, 1)
+
+    total(zred.at[0 : NZ - 1], ar_send.at[1], ar_recv.at[1]).wait_recv()
+    tot = zred[0]
     for k in range(1, NZ):
-        total = total + zred[k]
-    ag[pl.ds(2 * p_me, 2)] = total
-    ar_c = []
+        tot = tot + zred[k]
+    ag[pl.ds(2 * p_me, 2)] = tot
     for k in range(1, PLANE):
-        ar_c.append(send(
+        send(
             ag.at[pl.ds(2 * p_me, 2)], ag.at[pl.ds(2 * p_me, 2)],
-            ar_send.at[PLANE + NZ + k], ar_recv.at[PLANE + NZ + k], plane_dev[k - 1],
-        ))
-
-    for h in range(2):
-        qz.mid(h)
-    for h in range(2):
-        qz.end(h, to_e(ez, 2))
-    xs = []
-    for k in range(1, NX):
-        xs.append(send(
-            ez.at[x_pos[k - 1]], xz.at[k - 1],
-            z_send.at[2 * NZ + k], z_recv.at[2 * NZ + k], x_dev[k - 1],
-        ))
-
-    for c in ar_c:
-        c.wait_recv()
+            ar_send.at[2], ar_recv.at[2], plane_dev[k - 1],
+        )
+
+    total(pz, z_send.at[2], z_recv.at[2]).wait_recv()
+    t = hz[p_me].astype(F32)
+    for k in range(PLANE - 1):
+        t = t + pz[k].astype(F32)
+    gproj_o[:, 2 * third :] = t
+
+    total(ag.at[0 : 2 * PLANE - 2], ar_send.at[2], ar_recv.at[2]).wait_recv()
     for g in range(groups):
         for u in range(AUX // 8):
             tile = ag[g * (AUX // 8) + u]
@@ -532,20 +533,22 @@
         for j, o in ((taps_n, ggain_o), (taps_n + 1, gshift_o)):
             o[g : g + 1, :] = ag[(g * AUX + j) // 8, j % 8 : j % 8 + 1, :]
 
-    def last_sum(c, e, pos, r, copies):
-        for k in copies:
-            k.wait_recv()
-        t = e[pos].astype(F32)
-        for k in range(r.shape[0]):
-            t = t + r[k].astype(F32)
-        gproj_o[:, c * third : (c + 1) * third] = t
-
-    last_sum(0, ex, z, zx, zs[: NZ - 1])
-    last_sum(1, ey, z, zy, zs[NZ - 1 :])
-    last_sum(2, ez, x, xz, xs)
-
-    for c in sent:
+    for i, (e, zr) in enumerate(((ex, zx), (ey, zy))):
+        total(zr.at[0 : NZ - 1], z_send.at[i], z_recv.at[i]).wait_recv()
+        zr[z] = e[z]
+        t = zr[0].astype(F32)
+        for k in range(1, NZ):
+            t = t + zr[k].astype(F32)
+        gproj_o[:, i * third : (i + 1) * third] = t
+
+    for c in (c_st1, c_st2, c_halo, c_back):
         c.wait_send()
+    for q in (rx, ry, qx, qy, rz):
+        q.drain()
+    for i, ref in enumerate((red_r, zred.at[0 : NZ - 1], ag.at[0 : 2 * PLANE - 2])):
+        total(ref, ar_send.at[i], ar_recv.at[i]).wait_send()
+    for i, ref in enumerate((zx.at[0 : NZ - 1], zy.at[0 : NZ - 1], pz)):
+        total(ref, z_send.at[i], z_recv.at[i]).wait_send()
 
 
 def put_kernel(*refs):
@@ -570,17 +573,12 @@
     DMA = pltpu.SemaphoreType.DMA
 
     def color():
-        unit, small = (2, 16, 16, third), (2, 4, 16, third)
         return [
-            V((4, 2, 16, 16, third), BF16),
-            V(unit, BF16), V(unit, BF16), V(unit, BF16), V(unit, BF16),
-            V((4, 2, 4, 16, third), BF16),
-            V(small, BF16), V(small, BF16), V(small, BF16), V(small, BF16),
-            V((8, 16, third), BF16),
-            V((7, 16, third), BF16),
+            V((4, 2, 16, 16, third), BF16), V((3, 2, 16, 16, third), BF16), V((2, 16, 16, third), BF16),
+            V((4, 2, 4, 16, third), BF16), V((3, 2, 4, 16, third), BF16), V((2, 4, 16, third), BF16),
+            V((NZ, 16, third), BF16), V((NZ, 16, third), BF16),
         ]
 
-    tiny = (2, 2, 16, third)
     scratch = [
         V((rows, chans), BF16), V((rows, chans), BF16), V((rows, chans), BF16),
         V((taps_n, chans), BF16), V((groups, LANES), F32), V((groups, LANES), F32),
@@ -591,16 +589,11 @@
         V((groups, rows + HALO, LANES), F32), V((groups, rows + HALO, LANES), F32),
         V((groups, 32, LANES), F32),
         *color(), *color(),
-        V((8, 2, 8, 16, third), BF16),
-        V((2, 4, 8, 16, third), BF16), V((2, 3, 8, 16, third), BF16),
-        V((2, 3, 8, 16, third), BF16), V((2, 2, 8, 16, third), BF16),
-        V((4, 2, 2, 16, third), BF16),
-        V(tiny, BF16), V(tiny, BF16), V(tiny, BF16), V(tiny, BF16),
-        V((4, 16, third), BF16), V((3, 16, third), BF16),
-        V((32, 8, LANES), F32), V((PLANE - 1, 2, 8, LANES), F32), V((NZ, 2, 8, LANES), F32),
-        V((32, 8, LANES), F32),
-        DMA((4,)), DMA((4,)), DMA((44,)), DMA((44,)), DMA((2 * NZ + NX,)), DMA((2 * NZ + NX,)),
-        DMA((2 * PLANE + NZ,)), DMA((2 * PLANE + NZ,)),
+        V((NZ, 2, 8, 16, third), BF16), V((7, 2, 8, 16, third), BF16), V((5, 2, 8, 16, third), BF16),
+        V((PLANE, 16, third), BF16), V((PLANE - 1, 16, third), BF16),
+        V((2 * PLANE, 8, LANES), F32), V((PLANE - 1, 2, 8, LANES), F32), V((NZ, 2, 8, LANES), F32),
+        V((2 * PLANE, 8, LANES), F32),
+        DMA((4,)), DMA((4,)), DMA((5,)), DMA((38,)), DMA((3,)), DMA((3,)), DMA((3,)), DMA((3,)),
     ]
     S = jax.ShapeDtypeStruct
     shapes = (

time: 48.9 us -> 45.7 us (0.935)
  Pallas kernels: 48.2 us -> 44.9 us
    pallas_call x1, Pallas kernels: 47 us -> 43.7 us  [local(): pl.pallas_call(kernel, name='conv_backward', out_shape=shapes, in_specs=[...]
where the time goes in v3:
time: 45.7 us; the launch traced here: 45.6 us
  Pallas kernels  44.9 us (98%)
  between operations  0.64 us (1%)
    pallas_call x1, Pallas kernels, local(): pl.pallas_call(kernel, name='conv_backward', out_shape=shapes, in_specs=[...  43.7 us
    pallas_call x1, Pallas kernels, local(): pl.pallas_call(put_kernel, name='put_outputs', out_shape=shapes, in_specs...  1.23 us

profile of v3, /device:TPU:2, one launch (start us, length us, event | category | flops | bytes accessed | tf_op | source)
XLA Modules:
  0.0 45.6 jit_solution(13699668009856273543)
XLA Ops:
  0.6 43.7 %conv_backward.1 = (bf16[512,768]{1,0:T(8,128)(2,1)S(1)}, bf16[512,768]{1,0:T(8,128)(2,1)S(1)}, f32[31,768]{1,0:T(8,128)S(1)}, f32[6,128]{1,0:T(8,128)S(1)}, f32...) custom-call(bf16[512,768]{1,0:T(8,128)(2,1)} %value_h.1, bf16[512,768]{1,0:T(8,128)(2,1)} %gate_h.1, bf16[512,768]{1,0:T(8,128)(2,1)} %out_h.1, ...), custom_call_target="tpu_custom_call" | custom-call | tf_op jit(solution)/shard_map/conv_backward/pallas_call | solution.py:603
  44.3 1.2 %put_outputs.1 = (bf16[512,768]{1,0:T(8,128)(2,1)}, bf16[512,768]{1,0:T(8,128)(2,1)}, f32[31,768]{1,0:T(8,128)}, f32[6,128]{1,0:T(8,128)}, f32[6,128]{1,0:T(8,128)}, /*index=5*/f32[16,768]{1,0:T(8,128)}) custom-call(bf16[512,768]{1,0:T(8,128)(2,1)S(1)} %get-tuple-element.18.refs_0_, bf16[512,768]{1,0:T(8,128)(2,1)S(1)} %get-tuple-element.19.refs_1_, ...), custom_call_target="tpu_custom_call" | custom-call | tf_op jit(solution)/shard_map/put_outputs/pallas_call | solution.py:620

commit v4 on v3

--- a/solution.py
+++ b/solution.py
@@ -28,7 +28,7 @@
     value_h, gate_h, out_h, taps_h, gain_h, shift_h, weight_h, og_h,
     gv_v, gg_v, gtaps_o, ggain_o, gshift_o, gproj_o,
     value_v, gate_v, out_v, taps_v, gain_v, shift_v, weight_v, og_v, in_sem,
-    st_a, st_b, cen_b, inv_b, sum_b, dot_b, act_v, fac_v, sc_v, hg, gt, tapsf,
+    st_a, st_b, cen_b, inv_b, sum_b, dot_b, act_v, fac_v, sc_v, hg, gt, tapsf, edge, edge_r,
     gx, r_x, mx, hx, s_x, m2x, ex, zx,
     gy, r_y, my, hy, s_y, m2y, ey, zy,
     gz, r_z, mz, hz, pz,
@@ -45,6 +45,7 @@
     place = (z * NY + y) * NX + x
     last = NZ * PLANE
     blocks = rows // LANES
+    NB = 256
 
     def at_place(s):
         return {"sp_0": s // PLANE, "sp_1": lax.rem(s // NX, NY), "sp_2": lax.rem(s, NX)}
@@ -70,12 +71,23 @@
             src_ref=ref, dst_ref=ref, send_sem=ss, recv_sem=rs, device_id=other, device_id_type=MESH
         )
 
-    c_out = load(0, out_h, out_v)
+    def blk(i):
+        return slice(i * LANES, (i + 1) * LANES)
+
+    c_out = [load(8 + i, out_h.at[blk(i)], out_v.at[blk(i)]) for i in range(blocks)]
+    body, tail = slice(0, rows - HALO), slice(rows - HALO, rows)
+    c_tail = [
+        load(4, gate_h.at[tail], gate_v.at[tail]), load(5, value_h.at[tail], value_v.at[tail])
+    ]
     c_gain = load(1, gain_h, gain_v)
     c_shift = load(2, shift_h, shift_v)
     c_taps = load(3, taps_h, taps_v)
-    c_gate = load(4, gate_h, gate_v)
-    c_value = load(5, value_h, value_v)
+
+    c_og = load(6, og_h, og_v)
+    c_weight = [
+        load(n, weight_h.at[:, cs], weight_v.at[:, cs])
+        for n, cs in ((0, slice(0, NB)), (7, slice(NB, chans)))
+    ]
 
     barrier = pltpu.get_barrier_semaphore()
     p_me = y * NX + x
@@ -91,19 +103,20 @@
     for dev in partners:
         pl.semaphore_signal(barrier, inc=1, device_id=dev, device_id_type=MESH)
 
-    c_out.wait()
-    c_og = load(6, og_h, og_v)
+    c_out[0].wait()
+    c_body = [
+        load(12, gate_h.at[body], gate_v.at[body]), load(13, value_h.at[body], value_v.at[body])
+    ]
 
     def cols(g):
         return slice(g * LANES, (g + 1) * LANES)
-
-    def blk(i):
-        return slice(i * LANES, (i + 1) * LANES)
 
     eye = lax.broadcasted_iota(jnp.int32, (LANES, LANES), 0) == lax.broadcasted_iota(
         jnp.int32, (LANES, LANES), 1
     )
     for i in range(blocks):
+        if i:
+            c_out[i].wait()
         part = out_v[blk(i), cols(0)].astype(F32)
         for g in range(1, groups):
             part = part + out_v[blk(i), cols(g)].astype(F32)
@@ -121,26 +134,31 @@
     c_st1 = send(st_a.at[0], st_b.at[0], st_sem.at[0], st_sem.at[1], other)
 
     SB = 64
-    c_gate.wait()
-    c_value.wait()
-    c_weight = load(7, weight_h, weight_v)
-
-    @pl.loop(0, rows // SB)
-    def _(i):
-        rs = pl.ds(i * SB, SB)
+    def gate_rows(lo, n):
+        rs = pl.ds(lo, n)
         for g in range(groups):
             gated = value_v[rs, cols(g)].astype(F32) * sigmoid(gate_v[rs, cols(g)].astype(F32))
-            gt[g, pl.ds(HALO + i * SB, SB), :] = gated.astype(BF16).astype(F32)
-
+            gt[g, pl.ds(HALO + lo, n), :] = gated.astype(BF16).astype(F32)
+
+    for c in c_tail:
+        c.wait()
+    gate_rows(rows - HALO, HALO)
+    c_halo = send(
+        gt.at[:, pl.ds(rows, HALO), :], gt.at[:, pl.ds(0, HALO), :],
+        halo_sem.at[0], halo_sem.at[1], nxt,
+    )
     c_gain.wait()
     c_shift.wait()
     c_taps.wait()
     for g in range(groups):
         tapsf[g, 0:taps_n, :] = taps_v[:, cols(g)].astype(F32)
-    c_halo = send(
-        gt.at[:, pl.ds(rows, HALO), :], gt.at[:, pl.ds(0, HALO), :],
-        halo_sem.at[0], halo_sem.at[1], nxt,
-    )
+    def act_grad(n):
+        cs = pl.ds(pl.multiple_of(n * NB, NB), NB)
+        sc_v[:, cs] = jnp.dot(og_v[...], weight_v[:, cs], preferred_element_type=F32)
+
+    c_og.wait()
+    c_weight[0].wait()
+    act_grad(0)
     c_st1.wait_recv()
 
     def spread(dst, src):
@@ -162,10 +180,10 @@
         for g in range(groups):
             sh = (out_v[rs, cols(g)].astype(F32) - cen) * inv * gain_v[g : g + 1, :] + shift_v[g : g + 1, :]
             sg = sigmoid(sh)
-            act_v[rs, cols(g)] = (sh * sg).astype(BF16)
-            fac_v[rs, cols(g)] = sg * (1.0 + sh * (1.0 - sg))
-
-    c_og.wait()
+            act = sh * sg
+            act_v[rs, cols(g)] = act.astype(BF16)
+            fac_v[rs, cols(g)] = sg + act * (1.0 - sg)
+
     zb = PLANE * 16
     third = chans // 3
     HZ = NZ // 2
@@ -182,9 +200,14 @@
             for yy in range(NY):
                 for xx in range(NX):
                     r0 = zq * zb + (yy * NX + xx) * 16
-                    gx[xx, hf, yy * 4 + zq] = part[r0 : r0 + 16, 0:third]
-                    gy[yy, hf, xx * 4 + zq] = part[r0 : r0 + 16, third : 2 * third]
-                    gz[hf * ZM + zq, yy // 2, (yy % 2) * 4 + xx] = part[r0 : r0 + 16, 2 * third :]
+                    for c in range(third // LANES):
+                        piece = [
+                            part[r0 : r0 + 16, i * third + c * LANES : i * third + (c + 1) * LANES]
+                            for i in range(3)
+                        ]
+                        gx[xx, hf, yy * 4 + zq, c] = piece[0]
+                        gy[yy, hf, xx * 4 + zq, c] = piece[1]
+                        gz[hf * ZM + zq, yy // 2, (yy % 2) * 4 + xx, c] = piece[2]
 
     DIRS = (1, -1)
 
@@ -210,6 +233,9 @@
         def start(self, h):
             d = DIRS[h]
             self.go(h, self.g.at[lax.rem(self.pos + 2, 4), h], 0, d)
+
+        def single(self, h):
+            d = DIRS[h]
             self.go(h, self.g.at[lax.rem(self.pos + 4 - d, 4), h], 1, -d)
 
         def mid(self, h):
@@ -297,14 +323,12 @@
         ry.start(hf)
     for hf in range(2):
         rz.start(hf)
-
-    c_weight.wait()
-    NB = 256
-
-    @pl.loop(0, chans // NB)
-    def _(n):
-        cs = pl.ds(pl.multiple_of(n * NB, NB), NB)
-        sc_v[:, cs] = jnp.dot(og_v[...], weight_v[:, cs], preferred_element_type=F32)
+    for hf in range(2):
+        rx.single(hf)
+        ry.single(hf)
+
+    c_weight[1].wait()
+    pl.loop(1, chans // NB)(act_grad)
 
     zero = jnp.zeros((8, LANES), F32)
 
@@ -345,6 +369,10 @@
     for t in range(groups * AUX // 8, red.shape[0]):
         red[t] = zero
 
+    for c in c_body:
+        c.wait()
+    GB = 96
+    pl.loop(0, (rows - HALO) // GB)(lambda i: gate_rows(pl.multiple_of(i * GB, GB), GB))
     c_st2.wait_recv()
 
     both = (st_a[1] + st_b[1]) * (1.0 / chan_total)
@@ -360,10 +388,8 @@
             xc = (out_v[rs, cols(g)].astype(F32) - cen) * inv
             hg[g, rs, :] = inv * (sc_v[rs, cols(g)] - gs - xc * gd)
 
-    c_back = send(
-        hg.at[:, pl.ds(0, HALO), :], hg.at[:, pl.ds(rows, HALO), :],
-        halo_sem.at[2], halo_sem.at[3], prv,
-    )
+    for g in range(groups):
+        edge[g] = hg[g, 0:HALO, :].astype(BF16)
     rx.mid(0)
     ry.mid(0)
     for h in range(2):
@@ -376,22 +402,23 @@
         gt[:, 0:HALO, :] = jnp.zeros((groups, HALO, LANES), F32)
 
     UB = 8
+    UT = 16
 
     def taps_part(lo, hi):
         @pl.loop(lo, hi)
         def _(g):
             def step(t, acc):
-                base = pl.multiple_of(t * (8 * UB), 8 * UB)
-                hs = [hg[g, pl.ds(base + 8 * b, 8), :] for b in range(UB)]
+                base = pl.multiple_of(t * (8 * UT), 8 * UT)
+                hs = [hg[g, pl.ds(base + 8 * b, 8), :] for b in range(UT)]
                 acc = list(acc)
-                for o in range(taps_n + 8 * (UB - 1)):
+                for o in range(taps_n + 8 * (UT - 1)):
                     v = gt[g, pl.ds(base + (HALO - reach + o), 8), :]
-                    for b in range(UB):
+                    for b in range(UT):
                         if 0 <= o - 8 * b < taps_n:
                             acc[o - 8 * b] = acc[o - 8 * b] + hs[b] * v
                 return tuple(acc)
 
-            acc = lax.fori_loop(0, rows // (8 * UB), step, (zero,) * taps_n)
+            acc = lax.fori_loop(0, rows // (8 * UT), step, (zero,) * taps_n)
             for j in range(taps_n):
                 red[g * (AUX // 8) + j // 8, j % 8 : j % 8 + 1, :] = jnp.sum(
                     acc[j], axis=0, keepdims=True
@@ -400,12 +427,12 @@
     TB = 8 * UB
 
     def gated_part(lo, hi):
-        @pl.loop(lo, hi)
+        @pl.loop(0, groups)
         def _(g):
             weights = [jnp.broadcast_to(tapsf[g, j : j + 1, :], (8, LANES)) for j in range(taps_n)]
             cs = pl.ds(pl.multiple_of(g * LANES, LANES), LANES)
 
-            @pl.loop(0, rows // TB)
+            @pl.loop(lo, hi)
             def _(t):
                 base = pl.multiple_of(t * TB, TB)
                 parts = [None] * UB
@@ -443,12 +470,13 @@
             def _(p=p):
                 send(e.at[p], zr.at[z], z_send.at[i], z_recv.at[i], {"sp_0": p})
 
-    taps_part(0, 2)
+    taps_part(0, 1)
+    rx.mid(1)
+    ry.mid(1)
+    c_back = send(edge, edge_r, halo_sem.at[2], halo_sem.at[3], prv)
     for h in range(2):
         rz.short(h, 1)
-    rx.mid(1)
-    ry.mid(1)
-    taps_part(2, groups)
+    taps_part(1, groups)
     for k in range(1, PLANE):
         send(
             red.at[pl.ds(2 * plane_pos[k - 1], 2)], red_r.at[k - 1],
@@ -456,25 +484,23 @@
         )
     for h in range(2):
         rz.long(h, 2)
-    c_back.wait_recv()
-
-    @pl.when(place == last - 1)
-    def _():
-        hg[:, rows : rows + HALO, :] = jnp.zeros((groups, HALO, LANES), F32)
-
     gated_part(0, 1)
     rx.end(0, to_hx)
     qx.start(0)
+    qx.single(0)
     ry.end(0, to_hy)
     qy.start(0)
+    qy.single(0)
     for h in range(2):
         rz.short(h, 2)
     gated_part(1, 2)
     rx.end(1, to_hx)
     qx.start(1)
+    qx.single(1)
     ry.end(1, to_hy)
     qy.start(1)
-    gated_part(2, 4)
+    qy.single(1)
+    gated_part(2, 5)
     for h in range(2):
         rz.long(h, 3)
     qx.mid(0)
@@ -486,10 +512,14 @@
     zred[z] = mine
     for k in range(1, NZ):
         send(zred.at[z], zred.at[z], ar_send.at[1], ar_recv.at[1], z_dev[k - 1])
-    gated_part(4, 5)
+    gated_part(5, 6)
     qx.mid(1)
     qy.mid(1)
-    gated_part(5, groups)
+    gated_part(6, 7)
+    c_back.wait_recv()
+    for g in range(groups):
+        hg[g, rows : rows + HALO, :] = jnp.where(place == last - 1, 0.0, edge_r[g].astype(F32))
+    gated_part(7, 8)
     qx.end(0, to_e(ex))
     send_z(0, ex, zx, 0)
     qy.end(0, to_e(ey))
@@ -520,7 +550,11 @@
     t = hz[p_me].astype(F32)
     for k in range(PLANE - 1):
         t = t + pz[k].astype(F32)
-    gproj_o[:, 2 * third :] = t
+    def put_proj(i, t):
+        for c in range(third // LANES):
+            gproj_o[:, i * third + c * LANES : i * third + (c + 1) * LANES] = t[c]
+
+    put_proj(2, t)
 
     total(ag.at[0 : 2 * PLANE - 2], ar_send.at[2], ar_recv.at[2]).wait_recv()
     for g in range(groups):
@@ -539,7 +573,7 @@
         t = zr[0].astype(F32)
         for k in range(1, NZ):
             t = t + zr[k].astype(F32)
-        gproj_o[:, i * third : (i + 1) * third] = t
+        put_proj(i, t)
 
     for c in (c_st1, c_st2, c_halo, c_back):
         c.wait_send()
@@ -574,23 +608,23 @@
 
     def color():
         return [
-            V((4, 2, 16, 16, third), BF16), V((3, 2, 16, 16, third), BF16), V((2, 16, 16, third), BF16),
-            V((4, 2, 4, 16, third), BF16), V((3, 2, 4, 16, third), BF16), V((2, 4, 16, third), BF16),
-            V((NZ, 16, third), BF16), V((NZ, 16, third), BF16),
+            V((4, 2, 16, third // LANES, 16, LANES), BF16), V((3, 2, 16, third // LANES, 16, LANES), BF16), V((2, 16, third // LANES, 16, LANES), BF16),
+            V((4, 2, 4, third // LANES, 16, LANES), BF16), V((3, 2, 4, third // LANES, 16, LANES), BF16), V((2, 4, third // LANES, 16, LANES), BF16),
+            V((NZ, third // LANES, 16, LANES), BF16), V((NZ, third // LANES, 16, LANES), BF16),
         ]
 
     scratch = [
         V((rows, chans), BF16), V((rows, chans), BF16), V((rows, chans), BF16),
         V((taps_n, chans), BF16), V((groups, LANES), F32), V((groups, LANES), F32),
-        V((d_model, chans), BF16), V((rows, d_model), BF16), DMA((8,)),
+        V((d_model, chans), BF16), V((rows, d_model), BF16), DMA((14,)),
         V((2, 8, LANES), F32), V((2, 8, LANES), F32),
         *[V((rows, LANES), F32)] * 4,
         V((rows, chans), BF16), V((rows, chans), F32), V((rows, chans), F32),
         V((groups, rows + HALO, LANES), F32), V((groups, rows + HALO, LANES), F32),
-        V((groups, 32, LANES), F32),
+        V((groups, 32, LANES), F32), V((groups, HALO, LANES), BF16), V((groups, HALO, LANES), BF16),
         *color(), *color(),
-        V((NZ, 2, 8, 16, third), BF16), V((7, 2, 8, 16, third), BF16), V((5, 2, 8, 16, third), BF16),
-        V((PLANE, 16, third), BF16), V((PLANE - 1, 16, third), BF16),
+        V((NZ, 2, 8, third // LANES, 16, LANES), BF16), V((7, 2, 8, third // LANES, 16, LANES), BF16), V((5, 2, 8, third // LANES, 16, LANES), BF16),
+        V((PLANE, third // LANES, 16, LANES), BF16), V((PLANE - 1, third // LANES, 16, LANES), BF16),
         V((2 * PLANE, 8, LANES), F32), V((PLANE - 1, 2, 8, LANES), F32), V((NZ, 2, 8, LANES), F32),
         V((2 * PLANE, 8, LANES), F32),
         DMA((4,)), DMA((4,)), DMA((5,)), DMA((38,)), DMA((3,)), DMA((3,)), DMA((3,)), DMA((3,)),

time: 45.7 us -> 43.2 us (0.945)
  Pallas kernels: 44.9 us -> 42.5 us
    pallas_call x1, Pallas kernels: 43.7 us -> 41.3 us  [local(): pl.pallas_call(kernel, name='conv_backward', out_shape=shapes, in_specs=[...]
where the time goes in v4:
time: 43.2 us
  Pallas kernels  42.5 us (98%)
  between operations  0.64 us (1%)
    pallas_call x1, Pallas kernels, local(): pl.pallas_call(kernel, name='conv_backward', out_shape=shapes, in_specs=[...  41.3 us
    pallas_call x1, Pallas kernels, local(): pl.pallas_call(put_kernel, name='put_outputs', out_shape=shapes, in_specs...  1.23 us

profile of v4, /device:TPU:2, one launch (start us, length us, event | category | flops | bytes accessed | tf_op | source)
XLA Modules:
  0.0 43.2 jit_solution(11324844286248847175)
XLA Ops:
  0.6 41.3 %conv_backward.1 = (bf16[512,768]{1,0:T(8,128)(2,1)S(1)}, bf16[512,768]{1,0:T(8,128)(2,1)S(1)}, f32[31,768]{1,0:T(8,128)S(1)}, f32[6,128]{1,0:T(8,128)S(1)}, f32...) custom-call(bf16[512,768]{1,0:T(8,128)(2,1)} %value_h.1, bf16[512,768]{1,0:T(8,128)(2,1)} %gate_h.1, bf16[512,768]{1,0:T(8,128)(2,1)} %out_h.1, ...), custom_call_target="tpu_custom_call" | custom-call | tf_op jit(solution)/shard_map/conv_backward/pallas_call | solution.py:637
  41.9 1.2 %put_outputs.1 = (bf16[512,768]{1,0:T(8,128)(2,1)}, bf16[512,768]{1,0:T(8,128)(2,1)}, f32[31,768]{1,0:T(8,128)}, f32[6,128]{1,0:T(8,128)}, f32[6,128]{1,0:T(8,128)}, /*index=5*/f32[16,768]{1,0:T(8,128)}) custom-call(bf16[512,768]{1,0:T(8,128)(2,1)S(1)} %get-tuple-element.18.refs_0_, bf16[512,768]{1,0:T(8,128)(2,1)S(1)} %get-tuple-element.19.refs_1_, ...), custom_call_target="tpu_custom_call" | custom-call | tf_op jit(solution)/shard_map/put_outputs/pallas_call | solution.py:654

commit v5 on v4

--- a/solution.py
+++ b/solution.py
@@ -93,11 +93,13 @@
     p_me = y * NX + x
     plane_dev = []
     plane_pos = []
-    for k in range(1, PLANE):
-        p = lax.rem(p_me + k, PLANE)
-        plane_pos.append(p)
-        plane_dev.append({"sp_1": p // NX, "sp_2": lax.rem(p, NX)})
-    z_pos = [lax.rem(z + k, NZ) for k in range(1, NZ)]
+    offsets = [(i // NX, i % NX) for i in range(1, PLANE)]
+    offsets.sort(key=lambda o: -(min(o[0], NY - o[0]) + min(o[1], NX - o[1])))
+    for dy, dx in offsets:
+        py, px = lax.rem(y + dy, NY), lax.rem(x + dx, NX)
+        plane_pos.append(py * NX + px)
+        plane_dev.append({"sp_1": py, "sp_2": px})
+    z_pos = [lax.rem(z + k, NZ) for k in (4, 3, 5, 2, 6, 1, 7)]
     z_dev = [{"sp_0": p} for p in z_pos]
     partners = [other, nxt, prv] + plane_dev + z_dev
     for dev in partners:
@@ -161,9 +163,9 @@
     act_grad(0)
     c_st1.wait_recv()
 
-    def spread(dst, src):
-        for i in range(blocks):
-            dst[blk(i), :] = jnp.broadcast_to(src[i : i + 1, :], (LANES, LANES)).T
+    def spread(dst, src, first=0):
+        for i in range(src.shape[0]):
+            dst[blk(first + i), :] = jnp.broadcast_to(src[i : i + 1, :], (LANES, LANES)).T
 
     own, peer = st_a[0], st_b[0]
     s0, m0 = own[0:blocks], own[blocks : 2 * blocks]
@@ -352,11 +354,19 @@
         dot_b[rs, :] = r_dot
         return tuple(new)
 
-    sums = lax.fori_loop(0, rows // SB, norm_pass, (zero,) * (2 * groups))
-    for i in range(blocks):
-        st_a[1, i : i + 1, :] = jnp.sum(sum_b[blk(i), :].T, axis=0, keepdims=True)
-        st_a[1, blocks + i : blocks + i + 1, :] = jnp.sum(dot_b[blk(i), :].T, axis=0, keepdims=True)
-    c_st2 = send(st_a.at[1], st_b.at[1], st_sem.at[2], st_sem.at[3], other)
+    sums = (zero,) * (2 * groups)
+    hb = blocks // 2
+    hi = rows // SB // 2
+    c_st2 = []
+    for q in range(2):
+        sums = lax.fori_loop(q * hi, (q + 1) * hi, norm_pass, sums)
+        for i in range(hb):
+            k = q * hb + i
+            st_a[1 + q, i : i + 1, :] = jnp.sum(sum_b[blk(k), :].T, axis=0, keepdims=True)
+            st_a[1 + q, hb + i : hb + i + 1, :] = jnp.sum(dot_b[blk(k), :].T, axis=0, keepdims=True)
+        c_st2.append(send(
+            st_a.at[1 + q], st_b.at[1 + q], st_sem.at[2 + 2 * q], st_sem.at[3 + 2 * q], other
+        ))
 
     def put_row(g, j, row):
         red[(g * AUX + j) // 8, j % 8 : j % 8 + 1, :] = row
@@ -373,20 +383,20 @@
         c.wait()
     GB = 96
     pl.loop(0, (rows - HALO) // GB)(lambda i: gate_rows(pl.multiple_of(i * GB, GB), GB))
-    c_st2.wait_recv()
-
-    both = (st_a[1] + st_b[1]) * (1.0 / chan_total)
-    spread(sum_b, both[0:blocks])
-    spread(dot_b, both[blocks : 2 * blocks])
-
-    @pl.loop(0, rows // SB)
-    def _(i):
-        rs = pl.ds(i * SB, SB)
-        cen, inv = cen_b[rs, :], inv_b[rs, :]
-        gs, gd = sum_b[rs, :], dot_b[rs, :]
-        for g in range(groups):
-            xc = (out_v[rs, cols(g)].astype(F32) - cen) * inv
-            hg[g, rs, :] = inv * (sc_v[rs, cols(g)] - gs - xc * gd)
+    for q in range(2):
+        c_st2[q].wait_recv()
+        both = (st_a[1 + q] + st_b[1 + q]) * (1.0 / chan_total)
+        spread(sum_b, both[0:hb], q * hb)
+        spread(dot_b, both[hb : 2 * hb], q * hb)
+
+        @pl.loop(q * hi, (q + 1) * hi)
+        def _(i):
+            rs = pl.ds(i * SB, SB)
+            cen, inv = cen_b[rs, :], inv_b[rs, :]
+            gs, gd = sum_b[rs, :], dot_b[rs, :]
+            for g in range(groups):
+                xc = (out_v[rs, cols(g)].astype(F32) - cen) * inv
+                hg[g, rs, :] = inv * (sc_v[rs, cols(g)] - gs - xc * gd)
 
     for g in range(groups):
         edge[g] = hg[g, 0:HALO, :].astype(BF16)
@@ -500,11 +510,12 @@
     ry.end(1, to_hy)
     qy.start(1)
     qy.single(1)
-    gated_part(2, 5)
+    gated_part(2, 3)
     for h in range(2):
         rz.long(h, 3)
     qx.mid(0)
     qy.mid(0)
+    gated_part(3, 4)
     total(red_r, ar_send.at[0], ar_recv.at[0]).wait_recv()
     mine = red[pl.ds(2 * p_me, 2)]
     for k in range(PLANE - 1):
@@ -512,10 +523,10 @@
     zred[z] = mine
     for k in range(1, NZ):
         send(zred.at[z], zred.at[z], ar_send.at[1], ar_recv.at[1], z_dev[k - 1])
-    gated_part(5, 6)
+    gated_part(4, 5)
     qx.mid(1)
     qy.mid(1)
-    gated_part(6, 7)
+    gated_part(5, 7)
     c_back.wait_recv()
     for g in range(groups):
         hg[g, rows : rows + HALO, :] = jnp.where(place == last - 1, 0.0, edge_r[g].astype(F32))
@@ -575,7 +586,7 @@
             t = t + zr[k].astype(F32)
         put_proj(i, t)
 
-    for c in (c_st1, c_st2, c_halo, c_back):
+    for c in (c_st1, *c_st2, c_halo, c_back):
         c.wait_send()
     for q in (rx, ry, qx, qy, rz):
         q.drain()
@@ -617,7 +628,7 @@
         V((rows, chans), BF16), V((rows, chans), BF16), V((rows, chans), BF16),
         V((taps_n, chans), BF16), V((groups, LANES), F32), V((groups, LANES), F32),
         V((d_model, chans), BF16), V((rows, d_model), BF16), DMA((14,)),
-        V((2, 8, LANES), F32), V((2, 8, LANES), F32),
+        V((3, 8, LANES), F32), V((3, 8, LANES), F32),
         *[V((rows, LANES), F32)] * 4,
         V((rows, chans), BF16), V((rows, chans), F32), V((rows, chans), F32),
         V((groups, rows + HALO, LANES), F32), V((groups, rows + HALO, LANES), F32),
@@ -627,7 +638,7 @@
         V((PLANE, third // LANES, 16, LANES), BF16), V((PLANE - 1, third // LANES, 16, LANES), BF16),
         V((2 * PLANE, 8, LANES), F32), V((PLANE - 1, 2, 8, LANES), F32), V((NZ, 2, 8, LANES), F32),
         V((2 * PLANE, 8, LANES), F32),
-        DMA((4,)), DMA((4,)), DMA((5,)), DMA((38,)), DMA((3,)), DMA((3,)), DMA((3,)), DMA((3,)),
+        DMA((6,)), DMA((4,)), DMA((5,)), DMA((38,)), DMA((3,)), DMA((3,)), DMA((3,)), DMA((3,)),
     ]
     S = jax.ShapeDtypeStruct
     shapes = (

time: 43.2 us -> 42.4 us (0.981)
  Pallas kernels: 42.5 us -> 41.6 us
    pallas_call x1, Pallas kernels: 41.3 us -> 40.4 us  [local(): pl.pallas_call(kernel, name='conv_backward', out_shape=shapes, in_specs=[...]
where the time goes in v5:
time: 42.4 us; the launch traced here: 42.3 us
  Pallas kernels  41.6 us (98%)
  between operations  0.64 us (2%)
    pallas_call x1, Pallas kernels, local(): pl.pallas_call(kernel, name='conv_backward', out_shape=shapes, in_specs=[...  40.4 us
    pallas_call x1, Pallas kernels, local(): pl.pallas_call(put_kernel, name='put_outputs', out_shape=shapes, in_specs...  1.23 us

profile of v5, /device:TPU:2, one launch (start us, length us, event | category | flops | bytes accessed | tf_op | source)
XLA Modules:
  0.0 42.3 jit_solution(17753046110115892339)
XLA Ops:
  0.6 40.4 %conv_backward.1 = (bf16[512,768]{1,0:T(8,128)(2,1)S(1)}, bf16[512,768]{1,0:T(8,128)(2,1)S(1)}, f32[31,768]{1,0:T(8,128)S(1)}, f32[6,128]{1,0:T(8,128)S(1)}, f32...) custom-call(bf16[512,768]{1,0:T(8,128)(2,1)} %value_h.1, bf16[512,768]{1,0:T(8,128)(2,1)} %gate_h.1, bf16[512,768]{1,0:T(8,128)(2,1)} %out_h.1, ...), custom_call_target="tpu_custom_call" | custom-call | tf_op jit(solution)/shard_map/conv_backward/pallas_call | solution.py:648
  41.0 1.2 %put_outputs.1 = (bf16[512,768]{1,0:T(8,128)(2,1)}, bf16[512,768]{1,0:T(8,128)(2,1)}, f32[31,768]{1,0:T(8,128)}, f32[6,128]{1,0:T(8,128)}, f32[6,128]{1,0:T(8,128)}, /*index=5*/f32[16,768]{1,0:T(8,128)}) custom-call(bf16[512,768]{1,0:T(8,128)(2,1)S(1)} %get-tuple-element.18.refs_0_, bf16[512,768]{1,0:T(8,128)(2,1)S(1)} %get-tuple-element.19.refs_1_, ...), custom_call_target="tpu_custom_call" | custom-call | tf_op jit(solution)/shard_map/put_outputs/pallas_call | solution.py:665

commit v6 on v5

--- a/solution.py
+++ b/solution.py
@@ -135,7 +135,7 @@
     pl.semaphore_wait(barrier, len(partners))
     c_st1 = send(st_a.at[0], st_b.at[0], st_sem.at[0], st_sem.at[1], other)
 
-    SB = 64
+    SB = 128
     def gate_rows(lo, n):
         rs = pl.ds(lo, n)
         for g in range(groups):
@@ -192,24 +192,27 @@
 
     ZM = 4
 
-    def partial(hf):
+    def partial(hf, thirds):
         m = ZM * zb
-        lhs = og_v[:, hf * m : (hf + 1) * m]
+        lo = thirds[0] * third
         part = lax.dot_general(
-            lhs, act_v[...], (((0,), (0,)), ((), ())), preferred_element_type=F32
+            og_v[:, hf * m : (hf + 1) * m], act_v[:, lo : lo + len(thirds) * third],
+            (((0,), (0,)), ((), ())), preferred_element_type=F32,
         ).astype(BF16)
         for zq in range(ZM):
             for yy in range(NY):
                 for xx in range(NX):
                     r0 = zq * zb + (yy * NX + xx) * 16
                     for c in range(third // LANES):
-                        piece = [
-                            part[r0 : r0 + 16, i * third + c * LANES : i * third + (c + 1) * LANES]
-                            for i in range(3)
-                        ]
-                        gx[xx, hf, yy * 4 + zq, c] = piece[0]
-                        gy[yy, hf, xx * 4 + zq, c] = piece[1]
-                        gz[hf * ZM + zq, yy // 2, (yy % 2) * 4 + xx, c] = piece[2]
+                        for i in thirds:
+                            c0 = i * third - lo + c * LANES
+                            piece = part[r0 : r0 + 16, c0 : c0 + LANES]
+                            if i == 0:
+                                gx[xx, hf, yy * 4 + zq, c] = piece
+                            elif i == 1:
+                                gy[yy, hf, xx * 4 + zq, c] = piece
+                            else:
+                                gz[hf * ZM + zq, yy // 2, (yy % 2) * 4 + xx, c] = piece
 
     DIRS = (1, -1)
 
@@ -320,9 +323,11 @@
     rz = Ring8(24, 4)
 
     for hf in range(2):
-        partial(hf)
+        partial(hf, (0, 1))
         rx.start(hf)
         ry.start(hf)
+    for hf in range(2):
+        partial(hf, (2,))
     for hf in range(2):
         rz.start(hf)
     for hf in range(2):
@@ -384,6 +389,9 @@
     GB = 96
     pl.loop(0, (rows - HALO) // GB)(lambda i: gate_rows(pl.multiple_of(i * GB, GB), GB))
     for q in range(2):
+        if q:
+            rx.mid(0)
+            ry.mid(0)
         c_st2[q].wait_recv()
         both = (st_a[1 + q] + st_b[1 + q]) * (1.0 / chan_total)
         spread(sum_b, both[0:hb], q * hb)
@@ -400,8 +408,6 @@
 
     for g in range(groups):
         edge[g] = hg[g, 0:HALO, :].astype(BF16)
-    rx.mid(0)
-    ry.mid(0)
     for h in range(2):
         rz.long(h, 1)
 

time: 42.4 us -> 41 us (0.967)
  Pallas kernels: 41.6 us -> 40.2 us
    pallas_call x1, Pallas kernels: 40.4 us -> 39 us  [local(): pl.pallas_call(kernel, name='conv_backward', out_shape=shapes, in_specs=[...]
where the time goes in v6:
time: 41 us; the launch traced here: 40.8 us
  Pallas kernels  40.2 us (98%)
  between operations  0.64 us (2%)
    pallas_call x1, Pallas kernels, local(): pl.pallas_call(kernel, name='conv_backward', out_shape=shapes, in_specs=[...  39 us
    pallas_call x1, Pallas kernels, local(): pl.pallas_call(put_kernel, name='put_outputs', out_shape=shapes, in_specs...  1.23 us

profile of v6, /device:TPU:2, one launch (start us, length us, event | category | flops | bytes accessed | tf_op | source)
XLA Modules:
  0.0 40.8 jit_solution(2953104777832053199)
XLA Ops:
  0.6 39.0 %conv_backward.1 = (bf16[512,768]{1,0:T(8,128)(2,1)S(1)}, bf16[512,768]{1,0:T(8,128)(2,1)S(1)}, f32[31,768]{1,0:T(8,128)S(1)}, f32[6,128]{1,0:T(8,128)S(1)}, f32...) custom-call(bf16[512,768]{1,0:T(8,128)(2,1)} %value_h.1, bf16[512,768]{1,0:T(8,128)(2,1)} %gate_h.1, bf16[512,768]{1,0:T(8,128)(2,1)} %out_h.1, ...), custom_call_target="tpu_custom_call" | custom-call | tf_op jit(solution)/shard_map/conv_backward/pallas_call | solution.py:654
  39.6 1.2 %put_outputs.1 = (bf16[512,768]{1,0:T(8,128)(2,1)}, bf16[512,768]{1,0:T(8,128)(2,1)}, f32[31,768]{1,0:T(8,128)}, f32[6,128]{1,0:T(8,128)}, f32[6,128]{1,0:T(8,128)}, /*index=5*/f32[16,768]{1,0:T(8,128)}) custom-call(bf16[512,768]{1,0:T(8,128)(2,1)S(1)} %get-tuple-element.18.refs_0_, bf16[512,768]{1,0:T(8,128)(2,1)S(1)} %get-tuple-element.19.refs_1_, ...), custom_call_target="tpu_custom_call" | custom-call | tf_op jit(solution)/shard_map/put_outputs/pallas_call | solution.py:671
